TPU v7x, 32 devices: a whole 2x2x4 slice. The times are simulated.
32 devices in a mesh: sp: 8 (over z, y), dp: 4 (over x, core).
Axes of the slice: x: 2, y: 2, z: 4, core: 2. Of those that a mesh axis runs over, the one named last changes fastest.
Arguments:
- residual: bfloat16 [4, 1024, 2048], P('dp', 'sp'), may hold values from -6 to 6
- query: bfloat16 [4, 1024, 1536], P('dp', 'sp'), may hold values from -64 to 64
- latent: bfloat16 [4, 1024, 256], P('dp', 'sp'), may hold values from -6 to 6
- rope_key: bfloat16 [4, 1024, 32], P('dp', 'sp'), may hold values from -64 to 64
- latent_gain: float32 [256], replicated, may hold values from 0.1 to 1.9
- query_gain: float32 [96], replicated, may hold values from 0.7 to 5.6
- key_gain: float32 [96], replicated, may hold values from 0.7 to 5.6
- key_weight: bfloat16 [256, 1024], replicated, may hold values from -0.375 to 0.375
- value_weight: bfloat16 [256, 1024], replicated, may hold values from -0.375 to 0.375
- mix_gain: float32 [1024], replicated, may hold values from 0.1 to 1.9
- out_weight: bfloat16 [1024, 2048], replicated, may hold values from -0.1875 to 0.1875
- ffn_gain: float32 [2048], replicated, may hold values from 0.1 to 1.9
- expert_choice: int32 [4, 1024, 2], P('dp', 'sp'), may hold values from 0 to 31, as said below
- group_prob: float32 [4, 1024], P('dp', 'sp'), may hold values from 0.25 to 1
- expert_prob: float32 [4, 1024, 2], P('dp', 'sp'), may hold values from 0.05 to 1
- gate_weight: bfloat16 [32, 2048, 512], P(('sp', 'dp')), may hold values from -0.125 to 0.125
- up_weight: bfloat16 [32, 2048, 512], P(('sp', 'dp')), may hold values from -0.125 to 0.125
- down_weight: bfloat16 [32, 512, 2048], P(('sp', 'dp')), may hold values from -0.25 to 0.25
Outputs:
- layer_out: bfloat16 [4, 1024, 2048], P('dp', 'sp')
Inputs may be any that keep to these rules, and one draw needn't show every extreme that they name: `expert_choice`: A token's two experts differ and lie in one group of 8 consecutive expert numbers. In each aligned block of 128 tokens (the tokens of one device) no expert is named more than 16 times, and every expert of one group is named exactly 16 times in every block.
All inputs are finite; a program needn't handle non-finite values.
Results may differ from a plain program's by a relative error of at most 0.012.
The roundings to bfloat16 on the way count: a program that leaves them out, or rounds other values in their place, can miss the bound.
Values may be sent and summed in bfloat16 or wider, within the bound.
A program may use at most 64 MiB of HBM per device.

v0:
```python
import functools

import jax
import jax.numpy as jnp
from jax import lax
from jax.experimental import pallas as pl
from jax.experimental.pallas import tpu as pltpu
from jax.sharding import PartitionSpec as P

GROUPS = 4
SPAN = 64


eps = 1e-06


def angles(offset, span_count, rope_width):
    position = (offset + jnp.arange(span_count, dtype=jnp.int32)).astype(jnp.float32)
    frequency = 10000.0 ** (-2.0 * jnp.arange(rope_width // 2, dtype=jnp.float32) / rope_width)
    return position[:, None] * frequency[None, :]


def dot32(a, b):
    return jnp.dot(a, b, preferred_element_type=jnp.float32)


def dot_t(a, b):
    return lax.dot_general(a, b, (((0,), (0,)), ((), ())), preferred_element_type=jnp.float32)


def expert_kernel(
    n_y,
    n_dp,
    cap,
    rows,
    normed_ref,
    info_ref,
    pick_ref,
    stream_ref,
    gate_hbm,
    up_hbm,
    down_hbm,
    out_ref,
    gate_ref,
    up_ref,
    down_ref,
    out1,
    in1,
    out2,
    arrive,
    served,
    back2,
    merged,
    home,
    acc,
    w_sem,
    s1,
    r1,
    s2,
    r2,
    s3,
    r3,
    s4,
    r4,
    l_sem,
):
    peers = n_y * n_dp
    width = normed_ref.shape[1]
    sp = lax.axis_index("sp")
    dp = lax.axis_index("dp")
    plane = sp // n_y
    row = sp % n_y
    mine = row * n_dp + dp

    def column(k):
        return {"sp": ((plane + k) % GROUPS) * n_y + row, "dp": dp}

    def peer(j):
        other = (mine + j) % peers
        return {"sp": plane * n_y + other // n_dp, "dp": other % n_dp}

    loads = [
        pltpu.make_async_copy(gate_hbm, gate_ref, w_sem.at[0]),
        pltpu.make_async_copy(up_hbm, up_ref, w_sem.at[1]),
        pltpu.make_async_copy(down_hbm, down_ref, w_sem.at[2]),
    ]
    for load in loads:
        load.start()
    barrier = pltpu.get_barrier_semaphore()
    for k in range(1, GROUPS):
        pl.semaphore_signal(barrier, inc=1, device_id=column(k), device_id_type=pl.DeviceIdType.MESH)
    for j in range(1, peers):
        pl.semaphore_signal(barrier, inc=1, device_id=peer(j), device_id_type=pl.DeviceIdType.MESH)

    def remote(src, dst, send, recv, target):
        return pltpu.make_async_remote_copy(
            src_ref=src,
            dst_ref=dst,
            send_sem=send,
            recv_sem=recv,
            device_id=target,
            device_id_type=pl.DeviceIdType.MESH,
        )

    first = {}

    def pack(k, target):
        picks = pick_ref[(plane + k) % GROUPS]
        target[k, :, :width] = dot32(picks, normed_ref[...]).astype(jnp.bfloat16)
        target[k, :, width:] = dot32(picks, info_ref[...]).astype(jnp.bfloat16)

    for k in (2, 1, 3):
        pack(k, out1)
        if k == 2:
            pl.semaphore_wait(barrier, GROUPS - 1 + peers - 1)
        first[k] = remote(out1.at[k], in1.at[k], s1.at[k], r1.at[k], column(k))
        first[k].start()
    pack(0, in1)

    def slots(k):
        info = in1[k, :, width:].astype(jnp.float32)
        place = lax.broadcasted_iota(jnp.int32, (rows, peers * cap), 1).astype(jnp.float32)
        return place == info[:, 0:1], place == info[:, 1:2], info

    second = {}

    def scatter(k):
        if k:
            first[k].wait_recv()
        at0, at1, _ = slots(k)
        choose = (at0.astype(jnp.float32) + at1.astype(jnp.float32)).astype(jnp.bfloat16)
        placed = dot_t(choose, in1[k, :, :width]).astype(jnp.bfloat16)
        for e in range(peers):
            out2[k, e] = placed[e * cap : (e + 1) * cap]
        second[k] = [
            remote(
                out2.at[k, (mine + j) % peers], arrive.at[k, j], s2.at[k, j], r2.at[k, j], peer(j)
            )
            for j in range(1, peers)
        ]
        for copy in second[k]:
            copy.start()
        arrive[k, 0] = out2[k, mine]

    third = {}

    def serve(k):
        for copy in second[k]:
            copy.wait_recv()
        if k == 2:
            for load in loads:
                load.wait()
        given = arrive[k].reshape(peers * cap, width)
        gate_act = dot32(given, gate_ref[...])
        upward = dot32(given, up_ref[...])
        hidden = (gate_act * (1.0 / (1.0 + jnp.exp(-gate_act))) * upward).astype(jnp.bfloat16)
        result = dot32(hidden, down_ref[...]).astype(jnp.bfloat16)
        for j in range(peers):
            served[k, j] = result[j * cap : (j + 1) * cap]
        third[k] = [
            remote(
                served.at[k, j], back2.at[k, mine], s3.at[k, j], r3.at[k, peers - j], peer(peers - j)
            )
            for j in range(1, peers)
        ]
        for copy in third[k]:
            copy.start()
        back2[k, mine] = served[k, 0]

    fourth = {}

    def merge(k):
        for copy in third[k]:
            copy.wait_recv()
        at0, at1, info = slots(k)
        high = jnp.where(at0, info[:, 2:3], 0.0) + jnp.where(at1, info[:, 4:5], 0.0)
        low = jnp.where(at0, info[:, 3:4], 0.0) + jnp.where(at1, info[:, 5:6], 0.0)
        got = back2[k].reshape(peers * cap, width)
        total = dot32(high.astype(jnp.bfloat16), got) + dot32(low.astype(jnp.bfloat16), got)
        if k:
            merged[k] = total.astype(jnp.bfloat16)
            fourth[k] = remote(merged.at[k], home.at[k], s4.at[k], r4.at[k], column(GROUPS - k))
            fourth[k].start()
        else:
            acc[...] = stream_ref[...] + dot_t(pick_ref[plane], total.astype(jnp.bfloat16))

    scatter(0)
    scatter(2)
    scatter(1)
    scatter(3)
    serve(2)
    serve(1)
    serve(3)
    merge(2)
    merge(1)
    merge(3)
    serve(0)
    merge(0)
    for k in (2, 1, 3):
        fourth[k].wait_recv()
        acc[...] += dot_t(pick_ref[(plane + k) % GROUPS], home[k])
    out_ref[...] = acc[...].astype(jnp.bfloat16)
    for k in range(GROUPS):
        if k:
            first[k].wait_send()
            fourth[k].wait_send()
        for copy in second[k] + third[k]:
            copy.wait_send()


def attention_kernel(
    n_sp,
    n_y,
    heads,
    nope,
    rope,
    value_width,
    query_ref,
    packed_ref,
    latent_gain_ref,
    query_gain_ref,
    query_swap_ref,
    key_gain_ref,
    key_swap_ref,
    cos_ref,
    sin_ref,
    key_weight_ref,
    value_weight_ref,
    residual_ref,
    mix_gain_ref,
    ffn_gain_ref,
    out_weight_hbm,
    stream_ref,
    normed_ref,
    out_weight_ref,
    queries_in,
    packed_in,
    queries,
    keys,
    values,
    heads_out,
    token_in,
    mixed,
    w_sem,
    sq,
    rq,
    sz,
    rz,
    sy,
    ry,
    so,
    ro,
):
    bf = jnp.bfloat16
    tok = residual_ref.shape[0]
    length = n_sp * tok
    qk = nope + rope
    lat = packed_ref.shape[1]
    me = lax.axis_index("sp")
    plane = me // n_y
    row = me % n_y
    load = pltpu.make_async_copy(out_weight_hbm, out_weight_ref, w_sem.at[0])
    load.start()

    def remote(src, dst, send, recv, target):
        return pltpu.make_async_remote_copy(
            src_ref=src,
            dst_ref=dst,
            send_sem=send,
            recv_sem=recv,
            device_id={"sp": target},
            device_id_type=pl.DeviceIdType.MESH,
        )

    barrier = pltpu.get_barrier_semaphore()
    for j in range(1, n_sp):
        pl.semaphore_signal(
            barrier,
            inc=1,
            device_id={"sp": (me + j) % n_sp},
            device_id_type=pl.DeviceIdType.MESH,
        )
    pl.semaphore_wait(barrier, n_sp - 1)

    down = []
    for k in range(1, GROUPS):
        target = ((plane + k) % GROUPS) * n_y + row
        down.append(remote(packed_ref, packed_in.at[me], sz.at[k], rz.at[k], target))
        down[-1].start()
    across = []

    def spread(k, source):
        index = ((plane + GROUPS - k) % GROUPS) * n_y + row
        for m in range(1, n_y):
            target = plane * n_y + (row + m) % n_y
            across.append(remote(source, packed_in.at[index], sy.at[k, m], ry.at[k, m], target))
            across[-1].start()

    spread(0, packed_ref)
    sent = []
    for j in range(1, n_sp):
        target = (me + j) % n_sp
        sent.append(remote(query_ref.at[target], queries_in.at[me], sq.at[j], rq.at[j], target))
        sent[-1].start()
    packed_in[me] = packed_ref[...]
    queries_in[me] = query_ref[me]
    for k in range(1, GROUPS):
        down[k - 1].wait_recv()
        spread(k, packed_in.at[((plane + GROUPS - k) % GROUPS) * n_y + row])
    for copy in across:
        copy.wait_recv()

    def selector(rows, columns, source):
        i = lax.broadcasted_iota(jnp.int32, (rows, columns), 0)
        c = lax.broadcasted_iota(jnp.int32, (rows, columns), 1)
        return (i == source(c)).astype(jnp.float32).astype(bf)

    half = rope // 2

    def swapped(c):
        return jnp.where(c < nope, -1, jnp.where(c < nope + half, c + half, c - half))

    def shape_head(plain, turned, gain, swap_gain, rows):
        scale = lax.rsqrt(jnp.sum(plain * plain, axis=-1, keepdims=True) / qk + eps)
        return (
            plain * scale * gain * cos_ref[rows, :] + turned * scale * swap_gain * sin_ref[rows, :]
        ).astype(bf)

    strips = lat // rope
    strip_rows = tok // strips

    def prepare(s, carry):
        rows = pl.ds(pl.multiple_of(s * tok, tok), tok)
        block = packed_in[s]
        raw = block[:tok].astype(jnp.float32)
        scale = lax.rsqrt(jnp.mean(raw * raw, axis=-1, keepdims=True) + eps)
        latent = (raw * scale * latent_gain_ref[...]).astype(bf)
        values[rows, :] = dot32(latent, value_weight_ref[...]).astype(bf)
        part = dot32(latent, key_weight_ref[...]).astype(bf)
        tail = block[tok:]
        plain_rope = jnp.concatenate(
            [
                dot32(tail, selector(lat, qk, lambda c: jnp.where(c < nope, -1, c - nope + i * rope)))
                for i in range(strips)
            ],
            axis=0,
        )
        turned = jnp.concatenate(
            [
                dot32(
                    tail,
                    selector(
                        lat, qk, lambda c: jnp.where(c < nope, -1, swapped(c) - nope + i * rope)
                    ),
                )
                for i in range(strips)
            ],
            axis=0,
        )
        for h in range(heads):
            plain = plain_rope + dot32(
                part, selector(heads * nope, qk, lambda c: jnp.where(c < nope, c + h * nope, -1))
            )
            keys[h, rows, :] = shape_head(
                plain, turned, key_gain_ref[...], key_swap_ref[...], rows
            )
        return carry

    lax.fori_loop(0, n_sp, prepare, 0)
    for copy in sent:
        copy.wait_recv()

    def prepare_queries(s, carry):
        rows = pl.ds(pl.multiple_of(s * tok, tok), tok)
        raw = queries_in[s]
        for h in range(heads):
            plain = dot32(raw, selector(heads * qk, qk, lambda c: c + h * qk))
            turned = dot32(
                raw,
                selector(
                    heads * qk, qk, lambda c: jnp.where(c < nope, -1, swapped(c) + h * qk)
                ),
            )
            queries[h, rows, :] = shape_head(
                plain, turned, query_gain_ref[...], query_swap_ref[...], rows
            )
        return carry

    lax.fori_loop(0, n_sp, prepare_queries, 0)

    blocks = 4
    block_rows = length // blocks
    for b in range(blocks):
        first_row = b * block_rows
        last_row = first_row + block_rows
        total = None
        lane = lax.broadcasted_iota(jnp.int32, (block_rows, heads * value_width), 1)
        q_pos = first_row + lax.broadcasted_iota(jnp.int32, (block_rows, last_row), 0)
        k_pos = lax.broadcasted_iota(jnp.int32, (block_rows, last_row), 1)
        allowed = k_pos // SPAN <= q_pos // SPAN
        for h in range(heads):
            scores = lax.dot_general(
                queries[h, first_row:last_row],
                keys[h, :last_row],
                (((1,), (1,)), ((), ())),
                preferred_element_type=jnp.float32,
            ) * (qk ** (-0.5))
            scores = jnp.where(allowed, scores, -1e30)
            raised = jnp.exp(scores - jnp.max(scores, axis=-1, keepdims=True))
            row_sum = jnp.sum(raised, axis=-1, keepdims=True)
            mine = dot32(raised.astype(bf), values[:last_row]) / row_sum
            total = mine if total is None else jnp.where(lane < h * value_width, total, mine)
        total = total.astype(bf)
        for t in range(block_rows // tok):
            index = first_row // tok + t
            heads_out[index] = total[t * tok : (t + 1) * tok]

            @pl.when(index != me)
            def _():
                remote(
                    heads_out.at[index], token_in.at[me], so.at[index], ro.at[me], index
                ).start()

    token_in[me] = heads_out[me]
    load.wait()
    for j in range(1, n_sp):
        other = (me + j) % n_sp
        remote(
            heads_out.at[other], token_in.at[other], so.at[other], ro.at[other], other
        ).wait()
    wide = heads * value_width
    square = None
    for s in range(n_sp):
        piece = token_in[s].astype(jnp.float32)
        part = jnp.sum(piece * piece, axis=-1, keepdims=True)
        square = part if square is None else square + part
    scale = lax.rsqrt(square / (n_sp * wide) + eps)
    for s in range(n_sp):
        span = slice(s * wide, (s + 1) * wide)
        mixed[:, span] = (token_in[s].astype(jnp.float32) * scale * mix_gain_ref[:, span]).astype(bf)
    stream = residual_ref[...].astype(jnp.float32) + dot32(mixed[...], out_weight_ref[...])
    stream_ref[...] = stream
    scale = lax.rsqrt(jnp.mean(stream * stream, axis=-1, keepdims=True) + eps)
    normed_ref[...] = (stream * scale * ffn_gain_ref[...]).astype(bf)
    for copy in down + across + sent:
        copy.wait_send()


def attended(
    residual,
    query,
    latent,
    rope_key,
    latent_gain,
    query_gain,
    key_gain,
    key_weight,
    value_weight,
    mix_gain,
    out_weight,
    ffn_gain,
    head_count,
    nope,
    value_width,
):
    n_sp = lax.axis_size("sp")
    n_y = n_sp // GROUPS
    me = lax.axis_index("sp")
    tok, width = residual.shape
    rope = rope_key.shape[1]
    qk = nope + rope
    lat = latent.shape[1]
    heads = head_count // n_sp
    length = n_sp * tok
    half = rope // 2
    bf = jnp.bfloat16
    query_blocks = query.reshape(tok, n_sp, heads * qk).transpose(1, 0, 2)
    strips = lat // rope
    tail = rope_key.reshape(strips, tok // strips, rope).transpose(1, 0, 2).reshape(-1, lat)
    packed = jnp.concatenate([latent, tail], axis=0)
    phases = angles(0, length, rope)
    cos, sin = jnp.cos(phases), jnp.sin(phases)
    cos = jnp.concatenate([jnp.ones((length, nope), jnp.float32), cos, cos], axis=1)
    sin = jnp.concatenate([jnp.zeros((length, nope), jnp.float32), -sin, sin], axis=1)

    def swap(gain):
        return jnp.concatenate([gain[:nope], gain[nope + half :], gain[nope : nope + half]])

    key_own = lax.dynamic_slice_in_dim(key_weight, me * heads * nope, heads * nope, 1)
    value_own = lax.dynamic_slice_in_dim(value_weight, me * heads * value_width, heads * value_width, 1)
    vmem = pl.BlockSpec(memory_space=pltpu.VMEM)
    dma = pltpu.SemaphoreType.DMA
    wide = heads * value_width
    return pl.pallas_call(
        functools.partial(attention_kernel, n_sp, n_y, heads, nope, rope, value_width),
        out_shape=(
            jax.ShapeDtypeStruct((tok, width), jnp.float32),
            jax.ShapeDtypeStruct((tok, width), bf),
        ),
        in_specs=[vmem] * 14 + [pl.BlockSpec(memory_space=pl.ANY)],
        out_specs=(vmem, vmem),
        scratch_shapes=[
            pltpu.VMEM(out_weight.shape, bf),
            pltpu.VMEM((n_sp, tok, heads * qk), bf),
            pltpu.VMEM((n_sp,) + packed.shape, bf),
            pltpu.VMEM((heads, length, qk), bf),
            pltpu.VMEM((heads, length, qk), bf),
            pltpu.VMEM((length, wide), bf),
            pltpu.VMEM((n_sp, tok, wide), bf),
            pltpu.VMEM((n_sp, tok, wide), bf),
            pltpu.VMEM((tok, n_sp * wide), bf),
            dma((1,)),
            dma((n_sp,)),
            dma((n_sp,)),
            dma((GROUPS,)),
            dma((GROUPS,)),
            dma((GROUPS, n_y)),
            dma((GROUPS, n_y)),
            dma((n_sp,)),
            dma((n_sp,)),
        ],
        compiler_params=pltpu.CompilerParams(
            collective_id=1, has_side_effects=True, vmem_limit_bytes=48 * 1024 * 1024
        ),
    )(
        query_blocks,
        packed,
        latent_gain[None],
        query_gain[None],
        swap(query_gain)[None],
        key_gain[None],
        swap(key_gain)[None],
        cos,
        sin,
        key_own,
        value_own,
        residual,
        mix_gain[None],
        ffn_gain[None],
        out_weight,
    )


def routed(normed, stream, choice, group_prob, share, gate, up, down, expert_total):
    tok_rows, width = normed.shape
    n_y = lax.axis_size("sp") // GROUPS
    n_dp = lax.axis_size("dp")
    per_group = expert_total // GROUPS
    cap = tok_rows * GROUPS // expert_total
    rows = per_group * cap // choice.shape[1]
    group = choice[:, 0] // per_group
    order = jnp.arange(tok_rows, dtype=jnp.int32)
    before = order[None, :] < order[:, None]
    rank = jnp.sum((before & (group[None, :] == group[:, None])).astype(jnp.int32), axis=1)
    line = group * rows + rank
    pick = (
        (line[None, :] == jnp.arange(GROUPS * rows, dtype=jnp.int32)[:, None])
        .astype(jnp.bfloat16)
        .reshape(GROUPS, rows, tok_rows)
    )
    route = group_prob[:, None] * share / jnp.sum(share, axis=-1, keepdims=True)
    earlier = jnp.sum(
        (
            before[:, None, :, None] & (choice[:, :, None, None] == choice[None, None, :, :])
        ).astype(jnp.int32),
        axis=(2, 3),
    )
    position = (choice - group[:, None] * per_group) * cap + earlier
    high = lax.reduce_precision(route, 8, 7)
    low = route - high
    columns = jnp.concatenate(
        [
            position.astype(jnp.float32),
            jnp.stack([high[:, 0], low[:, 0], high[:, 1], low[:, 1]], axis=1),
            jnp.zeros((tok_rows, 122), jnp.float32),
        ],
        axis=1,
    ).astype(jnp.bfloat16)
    hidden = gate.shape[1]
    bf = jnp.bfloat16
    vmem = pl.BlockSpec(memory_space=pltpu.VMEM)
    hbm = pl.BlockSpec(memory_space=pl.ANY)
    dma = pltpu.SemaphoreType.DMA
    return pl.pallas_call(
        functools.partial(expert_kernel, n_y, n_dp, cap, rows),
        out_shape=jax.ShapeDtypeStruct((tok_rows, width), bf),
        in_specs=[vmem] * 4 + [hbm] * 3,
        out_specs=vmem,
        scratch_shapes=[
            pltpu.VMEM((width, hidden), bf),
            pltpu.VMEM((width, hidden), bf),
            pltpu.VMEM((hidden, width), bf),
            pltpu.VMEM((GROUPS, rows, width + 128), bf),
            pltpu.VMEM((GROUPS, rows, width + 128), bf),
            pltpu.VMEM((GROUPS, per_group, cap, width), bf),
            pltpu.VMEM((GROUPS, per_group, cap, width), bf),
            pltpu.VMEM((GROUPS, per_group, cap, width), bf),
            pltpu.VMEM((GROUPS, per_group, cap, width), bf),
            pltpu.VMEM((GROUPS, rows, width), bf),
            pltpu.VMEM((GROUPS, rows, width), bf),
            pltpu.VMEM((tok_rows, width), jnp.float32),
            dma((3,)),
            dma((GROUPS,)),
            dma((GROUPS,)),
            dma((GROUPS, per_group)),
            dma((GROUPS, per_group)),
            dma((GROUPS, per_group)),
            dma((GROUPS, per_group)),
            dma((GROUPS,)),
            dma((GROUPS,)),
            dma((1,)),
        ],
        compiler_params=pltpu.CompilerParams(
            collective_id=0, has_side_effects=True, vmem_limit_bytes=60 * 1024 * 1024
        ),
    )(normed, columns, pick, stream, gate, up, down)


def per_device(
    residual,
    query,
    latent,
    rope_key,
    latent_gain,
    query_gain,
    key_gain,
    key_weight,
    value_weight,
    mix_gain,
    out_weight,
    ffn_gain,
    expert_choice,
    group_prob,
    expert_prob,
    gate_weight,
    up_weight,
    down_weight,
):
    rope_width = rope_key.shape[2]
    qk_width = query_gain.shape[0]
    nope_width = qk_width - rope_width
    head_count = query.shape[2] // qk_width
    value_width = value_weight.shape[1] // head_count
    seq_devices = lax.axis_size("sp")
    stream, normed = attended(
        residual[0],
        query[0],
        latent[0],
        rope_key[0],
        latent_gain,
        query_gain,
        key_gain,
        key_weight,
        value_weight,
        mix_gain,
        out_weight,
        ffn_gain,
        head_count,
        nope_width,
        value_width,
    )
    expert_total = seq_devices * lax.axis_size("dp")
    return routed(
        normed,
        stream,
        expert_choice[0],
        group_prob[0],
        expert_prob[0],
        gate_weight[0],
        up_weight[0],
        down_weight[0],
        expert_total,
    )[None]


def solution(mesh):
    return jax.shard_map(
        per_device,
        mesh=mesh,
        in_specs=(
            P("dp", "sp", None),
            P("dp", "sp", None),
            P("dp", "sp", None),
            P("dp", "sp", None),
            P(),
            P(),
            P(),
            P(),
            P(),
            P(),
            P(),
            P(),
            P("dp", "sp", None),
            P("dp", "sp"),
            P("dp", "sp", None),
            P(("sp", "dp"), None, None),
            P(("sp", "dp"), None, None),
            P(("sp", "dp"), None, None),
        ),
        out_specs=P("dp", "sp", None),
        check_vma=False,
    )
```

profile of v0, /device:TPU:0, one launch (start us, length us, event | category | flops | bytes accessed | tf_op | source)
XLA Modules:
  0.0 120.4 jit_solution(17371675878835992024)
XLA Ops:
  0.0 0.0 copy-start.5
  0.0 0.0 copy-start.4
  0.0 0.0 copy-start.8
  0.0 1.9 %fusion = (f32[1024,16]{1,0:T(8,128)S(1)}, f32[1024,16]{1,0:T(8,128)S(1)}, f32[1024,16]{1,0:T(8,128)S(1)}) fusion(f32[16]{0:T(128)S(1)} %multiply_power_fusion, f32[1024]{0:T(1024)S(1)} %iota_convert_fusion), kind=kLoop, calls=%fused_computation.5 | loop fusion | flops 32768 | bytes 200768 | tf_op jit(solution)/shard_map/neg | solution.py:484
  2.0 0.0 copy-start.10
  2.0 0.0 copy-start.9
  2.0 0.0 copy-start.1
  2.0 0.0 copy-start.3
  2.0 0.0 copy-start.6
  2.1 0.0 copy-start.7
  2.1 0.6 pad_maximum_fusion
  2.7 0.9 constant_dynamic-slice_fusion
  3.6 0.0 copy-done.5
  3.6 0.1 fusion.8
  3.7 0.0 copy-done.4
  3.7 0.1 fusion.9
  3.7 0.1 maximum_bitcast_fusion
  3.8 0.0 copy-done.8
  3.8 0.2 copy.38
  4.1 0.2 copy.39
  4.3 0.1 copy.40
  4.4 0.1 reshape.85
  4.5 0.0 copy-done.1
  4.6 0.0 copy-done.3
  4.6 0.0 copy-done.6
  4.6 0.0 copy-done.7
  4.6 0.0 copy-start.12
  4.6 0.0 copy-start.11
  4.6 0.0 copy-start.13
  4.6 35.4 %shard_map.172 = (f32[128,2048]{1,0:T(8,128)S(1)}, bf16[128,2048]{1,0:T(8,128)(2,1)S(1)}) custom-call(bf16[8,128,192]{2,1,0:T(8,128)(2,1)S(1)} %bitcast.33, bf16[144,256]{1,0:T(8,128)(2,1)S(1)} %pad_maximum_fusion.2.packed_ref, f32[1,256]{1,0:T(1,128)S(1)} %bitcast.41, f32[1,96]{1,0:T(1,128)S(1)} %bitcast.37, f32[1,96]{1,0:T(1,128)S(1)} %get-tuple-element.29.query_swap_ref, ...), custom_call_target="tpu_custom_call" | custom-call | tf_op jit(solution)/shard_map/pallas_call | solution.py:494
  40.0 1.0 copy-done
  41.0 0.8 copy-done.2
  41.8 0.1 copy.43
  41.9 0.2 fusion.5
  42.1 0.1 subtract_multiply_fusion
  42.2 0.1 copy.47
  42.2 0.1 copy.45
  42.3 0.2 convert_reduce_fusion
  42.5 0.1 copy.49
  42.7 0.1 copy.48
  42.8 0.0 copy-done.13
  42.8 0.1 fusion.1
  42.9 0.1 fusion.6
  43.0 0.7 concatenate.24.info_ref
  43.8 0.2 convert_reduce_fusion.1
  44.0 0.7 compare_convert_fusion.pick_ref
  44.7 73.8 %shard_map.173 = bf16[128,2048]{1,0:T(8,128)(2,1)} custom-call(bf16[128,2048]{1,0:T(8,128)(2,1)} %copy-done.2, bf16[128,128]{1,0:T(8,128)(2,1)} %concatenate.24.info_ref, bf16[4,64,128]{2,1,0:T(8,128)(2,1)} %compare_convert_fusion.pick_ref, f32[128,2048]{1,0:T(8,128)} %copy-done, bf16[2048,512]{1,0:T(8,128)(2,1)} %bitcast.43, bf16[2048,512]{1,0:T(8,128)(2,1)} %bitcast.44, ...), custom_call_target="tpu_custom_call" | custom-call | tf_op jit(solution)/shard_map/pallas_call | solution.py:584
  118.5 1.9 %copy.51 = bf16[1,128,2048]{2,1,0:T(8,128)(2,1)} copy(bf16[1,128,2048]{2,1,0:T(8,128)(2,1)} %bitcast.42) | data formatting | bytes 1048576
  (21 shorter events, 0.2 us)
Async XLA Ops:
  0.0 3.6 %copy-start.5 = (f32[96]{0:T(128)S(1)}, f32[96]{0:T(128)}, u32[]{:S(2)}) copy-start(f32[96]{0:T(128)} %param.24) | copy-start | bytes 1156
  0.0 3.6 %copy-start.4 = (f32[96]{0:T(128)S(1)}, f32[96]{0:T(128)}, u32[]{:S(2)}) copy-start(f32[96]{0:T(128)} %param.23) | copy-start | bytes 1156
  0.0 3.8 %copy-start.8 = (bf16[1,128,1536]{2,1,0:T(8,128)(2,1)S(1)}, bf16[1,128,1536]{2,1,0:T(8,128)(2,1)}, u32[]{:S(2)}) copy-start(bf16[1,128,1536]{2,1,0:T(8,128)(2,1)} %param.19) | copy-start | bytes 1179652
  2.0 2.3 %copy-start.10 = (bf16[1,128,32]{1,2,0:T(8,128)(2,1)S(1)}, bf16[1,128,32]{1,2,0:T(8,128)(2,1)}, u32[]{:S(2)}) copy-start(bf16[1,128,32]{1,2,0:T(8,128)(2,1)} %param.21) | copy-start | bytes 24580
  2.0 2.5 %copy-start.9 = (bf16[1,128,256]{2,1,0:T(8,128)(2,1)S(1)}, bf16[1,128,256]{2,1,0:T(8,128)(2,1)}, u32[]{:S(2)}) copy-start(bf16[1,128,256]{2,1,0:T(8,128)(2,1)} %param.20) | copy-start | bytes 196612
  2.0 2.5 %copy-start.1 = (bf16[1,128,2048]{2,1,0:T(8,128)(2,1)S(1)}, bf16[1,128,2048]{2,1,0:T(8,128)(2,1)}, u32[]{:S(2)}) copy-start(bf16[1,128,2048]{2,1,0:T(8,128)(2,1)} %param.18) | copy-start | bytes 1572868
  2.0 2.5 %copy-start.3 = (f32[2048]{0:T(1024)S(1)}, f32[2048]{0:T(1024)}, u32[]{:S(2)}) copy-start(f32[2048]{0:T(1024)} %param.29) | copy-start | bytes 24580
  2.0 2.5 %copy-start.6 = (f32[1024]{0:T(1024)S(1)}, f32[1024]{0:T(1024)}, u32[]{:S(2)}) copy-start(f32[1024]{0:T(1024)} %param.27) | copy-start | bytes 12292
  2.1 2.5 %copy-start.7 = (f32[256]{0:T(256)S(1)}, f32[256]{0:T(256)}, u32[]{:S(2)}) copy-start(f32[256]{0:T(256)} %param.22) | copy-start | bytes 3076
  4.6 37.2 %copy-start.12 = (s32[1,128,2]{1,2,0:T(2,128)S(1)}, s32[1,128,2]{1,2,0:T(2,128)}, u32[]{:S(2)}) copy-start(s32[1,128,2]{1,2,0:T(2,128)} %param.30) | copy-start | bytes 3076
  4.6 38.1 %copy-start.11 = (f32[1,128,2]{1,2,0:T(2,128)S(1)}, f32[1,128,2]{1,2,0:T(2,128)}, u32[]{:S(2)}) copy-start(f32[1,128,2]{1,2,0:T(2,128)} %param.32) | copy-start | bytes 3076
  4.6 38.2 %copy-start.13 = (f32[1,128]{1,0:T(1,128)S(1)}, f32[1,128]{1,0:T(1,128)}, u32[]{:S(2)}) copy-start(f32[1,128]{1,0:T(1,128)} %param.31) | copy-start | bytes 1540
  40.0 1.0 copy-start
  41.0 0.8 copy-start.2
where the time goes:
time: 122 us; the launch traced here: 120 us
  Pallas kernels  109 us (89%)
  local copies, waits for them, and re-layouts  6.77 us (6%)
  other arithmetic  4.13 us (3%)
    pallas_call x1, Pallas kernels, routed(): pl.pallas_call(functools.partial(expert_kernel, n_y, n_dp, cap, rows), ou...  73.8 us
    pallas_call x1, Pallas kernels, attended(): pl.pallas_call(functools.partial(attention_kernel, n_sp, n_y, heads, nope...  35.4 us
    unnamed x33, local copies, waits for them, and re-layouts  4.28 us

commit v1 on v0

--- a/solution.py
+++ b/solution.py
@@ -44,6 +44,8 @@
     gate_ref,
     up_ref,
     down_ref,
+    notes_out,
+    notes,
     out1,
     in1,
     out2,
@@ -52,8 +54,9 @@
     back2,
     merged,
     home,
-    acc,
     w_sem,
+    s0,
+    r0,
     s1,
     r1,
     s2,
@@ -62,10 +65,11 @@
     r3,
     s4,
     r4,
-    l_sem,
 ):
+    bf = jnp.bfloat16
     peers = n_y * n_dp
-    width = normed_ref.shape[1]
+    chunks = in1.shape[1]
+    part = in1.shape[3]
     sp = lax.axis_index("sp")
     dp = lax.axis_index("dp")
     plane = sp // n_y
@@ -102,110 +106,145 @@
             device_id_type=pl.DeviceIdType.MESH,
         )
 
-    first = {}
-
-    def pack(k, target):
+    send_first = 1 + (plane + 1) // 2
+    send_last = GROUPS - 1 - 2 * (plane // 2)
+    send_order = (send_first, 6 - send_first - send_last, send_last)
+    recv_first = 6 - send_first - send_last
+    recv_last = 1 + 2 * (plane % 2)
+    recv_order = (recv_first, 6 - recv_first - recv_last, recv_last)
+
+    def span(c):
+        return slice(c * part, (c + 1) * part)
+
+    def note(k):
+        return remote(notes_out.at[k], notes.at[k], s0.at[k], r0.at[k], column(k))
+
+    def first(k, c):
+        return remote(out1.at[k, c], in1.at[k, c], s1.at[k, c], r1.at[k, c], column(k))
+
+    def second(k, c, j):
+        return remote(
+            out2.at[k, c, (mine + j) % peers],
+            arrive.at[k, c, j],
+            s2.at[k, c, j],
+            r2.at[k, c, j],
+            peer(j),
+        )
+
+    def third(k, c, j):
+        return remote(
+            served.at[k, c, j],
+            back2.at[k, c, mine],
+            s3.at[k, c, j],
+            r3.at[k, c, peers - j],
+            peer(peers - j),
+        )
+
+    def fourth(k, c):
+        return remote(merged.at[k, c], home.at[k, c], s4.at[k, c], r4.at[k, c], column(GROUPS - k))
+
+    for i, k in enumerate(send_order):
         picks = pick_ref[(plane + k) % GROUPS]
-        target[k, :, :width] = dot32(picks, normed_ref[...]).astype(jnp.bfloat16)
-        target[k, :, width:] = dot32(picks, info_ref[...]).astype(jnp.bfloat16)
-
-    for k in (2, 1, 3):
-        pack(k, out1)
-        if k == 2:
-            pl.semaphore_wait(barrier, GROUPS - 1 + peers - 1)
-        first[k] = remote(out1.at[k], in1.at[k], s1.at[k], r1.at[k], column(k))
-        first[k].start()
-    pack(0, in1)
+        notes_out[k] = dot32(picks, info_ref[...]).astype(bf)
+        for c in range(chunks):
+            out1[k, c] = dot32(picks, normed_ref[:, span(c)]).astype(bf)
+            if i == 0 and c == 0:
+                pl.semaphore_wait(barrier, GROUPS - 1 + peers - 1)
+            if c == 0:
+                note(k).start()
+            first(k, c).start()
+    own = pick_ref[plane]
+    notes[0] = dot32(own, info_ref[...]).astype(bf)
+    for c in range(chunks):
+        in1[0, c] = dot32(own, normed_ref[:, span(c)]).astype(bf)
 
     def slots(k):
-        info = in1[k, :, width:].astype(jnp.float32)
+        info = notes[k].astype(jnp.float32)
         place = lax.broadcasted_iota(jnp.int32, (rows, peers * cap), 1).astype(jnp.float32)
         return place == info[:, 0:1], place == info[:, 1:2], info
 
-    second = {}
-
-    def scatter(k):
-        if k:
-            first[k].wait_recv()
+    def scatter(k, local):
+        if not local:
+            note(k).wait_recv()
         at0, at1, _ = slots(k)
-        choose = (at0.astype(jnp.float32) + at1.astype(jnp.float32)).astype(jnp.bfloat16)
-        placed = dot_t(choose, in1[k, :, :width]).astype(jnp.bfloat16)
-        for e in range(peers):
-            out2[k, e] = placed[e * cap : (e + 1) * cap]
-        second[k] = [
-            remote(
-                out2.at[k, (mine + j) % peers], arrive.at[k, j], s2.at[k, j], r2.at[k, j], peer(j)
-            )
-            for j in range(1, peers)
-        ]
-        for copy in second[k]:
-            copy.start()
-        arrive[k, 0] = out2[k, mine]
-
-    third = {}
-
-    def serve(k):
-        for copy in second[k]:
-            copy.wait_recv()
-        if k == 2:
-            for load in loads:
-                load.wait()
-        given = arrive[k].reshape(peers * cap, width)
-        gate_act = dot32(given, gate_ref[...])
-        upward = dot32(given, up_ref[...])
-        hidden = (gate_act * (1.0 / (1.0 + jnp.exp(-gate_act))) * upward).astype(jnp.bfloat16)
-        result = dot32(hidden, down_ref[...]).astype(jnp.bfloat16)
-        for j in range(peers):
-            served[k, j] = result[j * cap : (j + 1) * cap]
-        third[k] = [
-            remote(
-                served.at[k, j], back2.at[k, mine], s3.at[k, j], r3.at[k, peers - j], peer(peers - j)
-            )
-            for j in range(1, peers)
-        ]
-        for copy in third[k]:
-            copy.start()
-        back2[k, mine] = served[k, 0]
-
-    fourth = {}
-
-    def merge(k):
-        for copy in third[k]:
-            copy.wait_recv()
+        choose = (at0.astype(jnp.float32) + at1.astype(jnp.float32)).astype(bf)
+        for c in range(chunks):
+            if not local:
+                first(k, c).wait_recv()
+            placed = dot_t(choose, in1[k, c]).astype(bf)
+            for e in range(peers):
+                out2[k, c, e] = placed[e * cap : (e + 1) * cap]
+            for j in range(1, peers):
+                second(k, c, j).start()
+            arrive[k, c, 0] = out2[k, c, mine]
+
+    def serve(k, load):
+        gate_act = None
+        for c in range(chunks):
+            for j in range(1, peers):
+                second(k, c, j).wait_recv()
+            if load and c == 0:
+                for copy in loads:
+                    copy.wait()
+            given = arrive[k, c].reshape(peers * cap, part)
+            gate_part = dot32(given, gate_ref[span(c), :])
+            up_part = dot32(given, up_ref[span(c), :])
+            gate_act = gate_part if gate_act is None else gate_act + gate_part
+            upward = up_part if c == 0 else upward + up_part
+        hidden = (gate_act * (1.0 / (1.0 + jnp.exp(-gate_act))) * upward).astype(bf)
+        for c in range(chunks):
+            result = dot32(hidden, down_ref[:, span(c)]).astype(bf)
+            for j in range(peers):
+                served[k, c, j] = result[j * cap : (j + 1) * cap]
+            for j in range(1, peers):
+                third(k, c, j).start()
+            back2[k, c, mine] = served[k, c, 0]
+
+    def merge(k, local):
         at0, at1, info = slots(k)
         high = jnp.where(at0, info[:, 2:3], 0.0) + jnp.where(at1, info[:, 4:5], 0.0)
         low = jnp.where(at0, info[:, 3:4], 0.0) + jnp.where(at1, info[:, 5:6], 0.0)
-        got = back2[k].reshape(peers * cap, width)
-        total = dot32(high.astype(jnp.bfloat16), got) + dot32(low.astype(jnp.bfloat16), got)
-        if k:
-            merged[k] = total.astype(jnp.bfloat16)
-            fourth[k] = remote(merged.at[k], home.at[k], s4.at[k], r4.at[k], column(GROUPS - k))
-            fourth[k].start()
-        else:
-            acc[...] = stream_ref[...] + dot_t(pick_ref[plane], total.astype(jnp.bfloat16))
-
-    scatter(0)
-    scatter(2)
-    scatter(1)
-    scatter(3)
-    serve(2)
-    serve(1)
-    serve(3)
-    merge(2)
-    merge(1)
-    merge(3)
-    serve(0)
-    merge(0)
-    for k in (2, 1, 3):
-        fourth[k].wait_recv()
-        acc[...] += dot_t(pick_ref[(plane + k) % GROUPS], home[k])
-    out_ref[...] = acc[...].astype(jnp.bfloat16)
+        high = high.astype(bf)
+        low = low.astype(bf)
+        for c in range(chunks):
+            for j in range(1, peers):
+                third(k, c, j).wait_recv()
+            got = back2[k, c].reshape(peers * cap, part)
+            total = (dot32(high, got) + dot32(low, got)).astype(bf)
+            if local:
+                home[0, c] = total
+            else:
+                merged[k, c] = total
+                fourth(k, c).start()
+
+    scatter(0, True)
+    scatter(recv_order[0], False)
+    serve(recv_order[0], True)
+    serve(0, False)
+    scatter(recv_order[1], False)
+    merge(recv_order[0], False)
+    serve(recv_order[1], False)
+    scatter(recv_order[2], False)
+    merge(recv_order[1], False)
+    serve(recv_order[2], False)
+    merge(0, True)
+    merge(recv_order[2], False)
+    for c in range(chunks):
+        total = stream_ref[:, span(c)] + dot_t(own, home[0, c])
+        for k in send_order:
+            fourth(k, c).wait_recv()
+            total = total + dot_t(pick_ref[(plane + k) % GROUPS], home[k, c])
+        out_ref[:, span(c)] = total.astype(bf)
     for k in range(GROUPS):
         if k:
-            first[k].wait_send()
-            fourth[k].wait_send()
-        for copy in second[k] + third[k]:
-            copy.wait_send()
+            note(k).wait_send()
+        for c in range(chunks):
+            if k:
+                first(k, c).wait_send()
+                fourth(k, c).wait_send()
+            for j in range(1, peers):
+                second(k, c, j).wait_send()
+                third(k, c, j).wait_send()
 
 
 def attention_kernel(
@@ -577,6 +616,8 @@
         axis=1,
     ).astype(jnp.bfloat16)
     hidden = gate.shape[1]
+    chunks = 4
+    part = width // chunks
     bf = jnp.bfloat16
     vmem = pl.BlockSpec(memory_space=pltpu.VMEM)
     hbm = pl.BlockSpec(memory_space=pl.ANY)
@@ -590,25 +631,27 @@
             pltpu.VMEM((width, hidden), bf),
             pltpu.VMEM((width, hidden), bf),
             pltpu.VMEM((hidden, width), bf),
-            pltpu.VMEM((GROUPS, rows, width + 128), bf),
-            pltpu.VMEM((GROUPS, rows, width + 128), bf),
-            pltpu.VMEM((GROUPS, per_group, cap, width), bf),
-            pltpu.VMEM((GROUPS, per_group, cap, width), bf),
-            pltpu.VMEM((GROUPS, per_group, cap, width), bf),
-            pltpu.VMEM((GROUPS, per_group, cap, width), bf),
-            pltpu.VMEM((GROUPS, rows, width), bf),
-            pltpu.VMEM((GROUPS, rows, width), bf),
-            pltpu.VMEM((tok_rows, width), jnp.float32),
+            pltpu.VMEM((GROUPS, rows, 128), bf),
+            pltpu.VMEM((GROUPS, rows, 128), bf),
+            pltpu.VMEM((GROUPS, chunks, rows, part), bf),
+            pltpu.VMEM((GROUPS, chunks, rows, part), bf),
+            pltpu.VMEM((GROUPS, chunks, per_group, cap, part), bf),
+            pltpu.VMEM((GROUPS, chunks, per_group, cap, part), bf),
+            pltpu.VMEM((GROUPS, chunks, per_group, cap, part), bf),
+            pltpu.VMEM((GROUPS, chunks, per_group, cap, part), bf),
+            pltpu.VMEM((GROUPS, chunks, rows, part), bf),
+            pltpu.VMEM((GROUPS, chunks, rows, part), bf),
             dma((3,)),
             dma((GROUPS,)),
             dma((GROUPS,)),
-            dma((GROUPS, per_group)),
-            dma((GROUPS, per_group)),
-            dma((GROUPS, per_group)),
-            dma((GROUPS, per_group)),
-            dma((GROUPS,)),
-            dma((GROUPS,)),
-            dma((1,)),
+            dma((GROUPS, chunks)),
+            dma((GROUPS, chunks)),
+            dma((GROUPS, chunks, per_group)),
+            dma((GROUPS, chunks, per_group)),
+            dma((GROUPS, chunks, per_group)),
+            dma((GROUPS, chunks, per_group)),
+            dma((GROUPS, chunks)),
+            dma((GROUPS, chunks)),
         ],
         compiler_params=pltpu.CompilerParams(
             collective_id=0, has_side_effects=True, vmem_limit_bytes=60 * 1024 * 1024

time: 122 us -> 132 us (1.082)
  Pallas kernels: 109 us -> 120 us
    pallas_call x1, Pallas kernels: 73.8 us -> 85 us  [routed(): pl.pallas_call(functools.partial(expert_kernel, n_y, n_dp, cap, rows), ou...]
where the time goes in v1:
time: 132 us
  Pallas kernels  120 us (91%)
  local copies, waits for them, and re-layouts  6.77 us (5%)
  other arithmetic  4.13 us (3%)
    pallas_call x1, Pallas kernels, routed(): pl.pallas_call(functools.partial(expert_kernel, n_y, n_dp, cap, rows), ou...  85 us
    pallas_call x1, Pallas kernels, attended(): pl.pallas_call(functools.partial(attention_kernel, n_sp, n_y, heads, nope...  35.4 us
    unnamed x33, local copies, waits for them, and re-layouts  4.28 us

profile of v1, /device:TPU:0, one launch (start us, length us, event | category | flops | bytes accessed | tf_op | source)
XLA Modules:
  0.0 131.6 jit_solution(4360995622451873366)
XLA Ops:
  0.0 0.0 copy-start.5
  0.0 0.0 copy-start.4
  0.0 0.0 copy-start.8
  0.0 1.9 %fusion = (f32[1024,16]{1,0:T(8,128)S(1)}, f32[1024,16]{1,0:T(8,128)S(1)}, f32[1024,16]{1,0:T(8,128)S(1)}) fusion(f32[16]{0:T(128)S(1)} %multiply_power_fusion, f32[1024]{0:T(1024)S(1)} %iota_convert_fusion), kind=kLoop, calls=%fused_computation.5 | loop fusion | flops 32768 | bytes 200768 | tf_op jit(solution)/shard_map/neg | solution.py:523
  2.0 0.0 copy-start.10
  2.0 0.0 copy-start.9
  2.0 0.0 copy-start.1
  2.0 0.0 copy-start.3
  2.0 0.0 copy-start.6
  2.1 0.0 copy-start.7
  2.1 0.6 pad_maximum_fusion
  2.7 0.9 constant_dynamic-slice_fusion
  3.6 0.0 copy-done.5
  3.6 0.1 fusion.8
  3.7 0.1 fusion.9
  3.7 0.1 maximum_bitcast_fusion
  3.8 0.0 copy-done.8
  3.8 0.2 copy.38
  4.1 0.2 copy.39
  4.3 0.1 copy.40
  4.4 0.1 reshape.85
  4.5 0.0 copy-done.1
  4.6 0.0 copy-done.3
  4.6 0.0 copy-done.6
  4.6 0.0 copy-done.7
  4.6 0.0 copy-start.12
  4.6 0.0 copy-start.11
  4.6 0.0 copy-start.13
  4.6 35.4 %shard_map.172 = (f32[128,2048]{1,0:T(8,128)S(1)}, bf16[128,2048]{1,0:T(8,128)(2,1)S(1)}) custom-call(bf16[8,128,192]{2,1,0:T(8,128)(2,1)S(1)} %bitcast.33, bf16[144,256]{1,0:T(8,128)(2,1)S(1)} %pad_maximum_fusion.2.packed_ref, f32[1,256]{1,0:T(1,128)S(1)} %bitcast.41, f32[1,96]{1,0:T(1,128)S(1)} %bitcast.37, f32[1,96]{1,0:T(1,128)S(1)} %get-tuple-element.29.query_swap_ref, ...), custom_call_target="tpu_custom_call" | custom-call | tf_op jit(solution)/shard_map/pallas_call | solution.py:533
  40.0 0.0 copy-start
  40.0 1.0 copy-done
  41.0 0.8 copy-done.2
  41.8 0.1 copy.43
  41.9 0.2 fusion.5
  42.1 0.1 subtract_multiply_fusion
  42.2 0.1 copy.47
  42.2 0.1 copy.45
  42.4 0.2 convert_reduce_fusion
  42.6 0.1 copy.49
  42.7 0.1 copy.48
  42.8 0.0 copy-done.13
  42.8 0.1 fusion.1
  42.9 0.1 fusion.6
  43.1 0.7 concatenate.24.info_ref
  43.8 0.2 convert_reduce_fusion.1
  44.0 0.7 compare_convert_fusion.pick_ref
  44.7 85.0 %shard_map.173 = bf16[128,2048]{1,0:T(8,128)(2,1)} custom-call(bf16[128,2048]{1,0:T(8,128)(2,1)} %copy-done.2, bf16[128,128]{1,0:T(8,128)(2,1)} %concatenate.24.info_ref, bf16[4,64,128]{2,1,0:T(8,128)(2,1)} %compare_convert_fusion.pick_ref, f32[128,2048]{1,0:T(8,128)} %copy-done, bf16[2048,512]{1,0:T(8,128)(2,1)} %bitcast.43, bf16[2048,512]{1,0:T(8,128)(2,1)} %bitcast.44, ...), custom_call_target="tpu_custom_call" | custom-call | tf_op jit(solution)/shard_map/pallas_call | solution.py:625
  129.7 1.9 %copy.51 = bf16[1,128,2048]{2,1,0:T(8,128)(2,1)} copy(bf16[1,128,2048]{2,1,0:T(8,128)(2,1)} %bitcast.42) | data formatting | bytes 1048576
  (21 shorter events, 0.2 us)
Async XLA Ops:
  0.0 3.6 %copy-start.5 = (f32[96]{0:T(128)S(1)}, f32[96]{0:T(128)}, u32[]{:S(2)}) copy-start(f32[96]{0:T(128)} %param.24) | copy-start | bytes 1156
  0.0 3.6 %copy-start.4 = (f32[96]{0:T(128)S(1)}, f32[96]{0:T(128)}, u32[]{:S(2)}) copy-start(f32[96]{0:T(128)} %param.23) | copy-start | bytes 1156
  0.0 3.8 %copy-start.8 = (bf16[1,128,1536]{2,1,0:T(8,128)(2,1)S(1)}, bf16[1,128,1536]{2,1,0:T(8,128)(2,1)}, u32[]{:S(2)}) copy-start(bf16[1,128,1536]{2,1,0:T(8,128)(2,1)} %param.19) | copy-start | bytes 1179652
  2.0 2.3 %copy-start.10 = (bf16[1,128,32]{1,2,0:T(8,128)(2,1)S(1)}, bf16[1,128,32]{1,2,0:T(8,128)(2,1)}, u32[]{:S(2)}) copy-start(bf16[1,128,32]{1,2,0:T(8,128)(2,1)} %param.21) | copy-start | bytes 24580
  2.0 2.5 %copy-start.9 = (bf16[1,128,256]{2,1,0:T(8,128)(2,1)S(1)}, bf16[1,128,256]{2,1,0:T(8,128)(2,1)}, u32[]{:S(2)}) copy-start(bf16[1,128,256]{2,1,0:T(8,128)(2,1)} %param.20) | copy-start | bytes 196612
  2.0 2.5 %copy-start.1 = (bf16[1,128,2048]{2,1,0:T(8,128)(2,1)S(1)}, bf16[1,128,2048]{2,1,0:T(8,128)(2,1)}, u32[]{:S(2)}) copy-start(bf16[1,128,2048]{2,1,0:T(8,128)(2,1)} %param.18) | copy-start | bytes 1572868
  2.0 2.5 %copy-start.3 = (f32[2048]{0:T(1024)S(1)}, f32[2048]{0:T(1024)}, u32[]{:S(2)}) copy-start(f32[2048]{0:T(1024)} %param.29) | copy-start | bytes 24580
  2.0 2.5 %copy-start.6 = (f32[1024]{0:T(1024)S(1)}, f32[1024]{0:T(1024)}, u32[]{:S(2)}) copy-start(f32[1024]{0:T(1024)} %param.27) | copy-start | bytes 12292
  2.1 2.5 %copy-start.7 = (f32[256]{0:T(256)S(1)}, f32[256]{0:T(256)}, u32[]{:S(2)}) copy-start(f32[256]{0:T(256)} %param.22) | copy-start | bytes 3076
  4.6 37.2 %copy-start.12 = (s32[1,128,2]{1,2,0:T(2,128)S(1)}, s32[1,128,2]{1,2,0:T(2,128)}, u32[]{:S(2)}) copy-start(s32[1,128,2]{1,2,0:T(2,128)} %param.30) | copy-start | bytes 3076
  4.6 38.1 %copy-start.11 = (f32[1,128,2]{1,2,0:T(2,128)S(1)}, f32[1,128,2]{1,2,0:T(2,128)}, u32[]{:S(2)}) copy-start(f32[1,128,2]{1,2,0:T(2,128)} %param.32) | copy-start | bytes 3076
  4.6 38.2 %copy-start.13 = (f32[1,128]{1,0:T(1,128)S(1)}, f32[1,128]{1,0:T(1,128)}, u32[]{:S(2)}) copy-start(f32[1,128]{1,0:T(1,128)} %param.31) | copy-start | bytes 1540
  40.0 1.0 copy-start
  41.0 0.8 copy-start.2

commit v2 on v1

--- a/solution.py
+++ b/solution.py
@@ -219,16 +219,16 @@
 
     scatter(0, True)
     scatter(recv_order[0], False)
+    scatter(recv_order[1], False)
     serve(recv_order[0], True)
-    serve(0, False)
-    scatter(recv_order[1], False)
+    serve(recv_order[1], False)
     merge(recv_order[0], False)
-    serve(recv_order[1], False)
     scatter(recv_order[2], False)
     merge(recv_order[1], False)
     serve(recv_order[2], False)
+    serve(0, False)
+    merge(recv_order[2], False)
     merge(0, True)
-    merge(recv_order[2], False)
     for c in range(chunks):
         total = stream_ref[:, span(c)] + dot_t(own, home[0, c])
         for k in send_order:
@@ -255,51 +255,73 @@
     rope,
     value_width,
     query_ref,
-    packed_ref,
+    latent_ref,
+    rope_ref,
     latent_gain_ref,
-    query_gain_ref,
-    query_swap_ref,
-    key_gain_ref,
-    key_swap_ref,
-    cos_ref,
-    sin_ref,
-    key_weight_ref,
-    value_weight_ref,
+    gain_ref,
+    rope_gain_ref,
+    trig_ref,
     residual_ref,
     mix_gain_ref,
     ffn_gain_ref,
+    key_weight_hbm,
+    value_weight_hbm,
     out_weight_hbm,
     stream_ref,
     normed_ref,
+    key_weight_ref,
+    value_weight_ref,
     out_weight_ref,
-    queries_in,
-    packed_in,
+    turned,
+    packed,
     queries,
-    keys,
     values,
+    top,
+    acc,
     heads_out,
-    token_in,
-    mixed,
     w_sem,
-    sq,
-    rq,
     sz,
     rz,
     sy,
     ry,
-    so,
-    ro,
 ):
     bf = jnp.bfloat16
+    f32 = jnp.float32
     tok = residual_ref.shape[0]
-    length = n_sp * tok
     qk = nope + rope
-    lat = packed_ref.shape[1]
+    half = rope // 2
+    lat = latent_ref.shape[1]
+    wide = 2 * value_width
+    chunk = n_y * tok
     me = lax.axis_index("sp")
     plane = me // n_y
     row = me % n_y
-    load = pltpu.make_async_copy(out_weight_hbm, out_weight_ref, w_sem.at[0])
-    load.start()
+    loads = [
+        pltpu.make_async_copy(key_weight_hbm, key_weight_ref, w_sem.at[0]),
+        pltpu.make_async_copy(value_weight_hbm, value_weight_ref, w_sem.at[1]),
+        pltpu.make_async_copy(out_weight_hbm, out_weight_ref, w_sem.at[2]),
+    ]
+    for load in loads:
+        load.start()
+
+    def at(index_plane, index_row):
+        return {"sp": index_plane * n_y + index_row}
+
+    barrier = pltpu.get_barrier_semaphore()
+    for k in range(1, GROUPS):
+        pl.semaphore_signal(
+            barrier,
+            inc=1,
+            device_id=at((plane + k) % GROUPS, row),
+            device_id_type=pl.DeviceIdType.MESH,
+        )
+    for m in range(1, n_y):
+        pl.semaphore_signal(
+            barrier,
+            inc=1,
+            device_id=at(plane, (row + m) % n_y),
+            device_id_type=pl.DeviceIdType.MESH,
+        )
 
     def remote(src, dst, send, recv, target):
         return pltpu.make_async_remote_copy(
@@ -307,182 +329,181 @@
             dst_ref=dst,
             send_sem=send,
             recv_sem=recv,
-            device_id={"sp": target},
+            device_id=target,
             device_id_type=pl.DeviceIdType.MESH,
         )
 
-    barrier = pltpu.get_barrier_semaphore()
-    for j in range(1, n_sp):
-        pl.semaphore_signal(
-            barrier,
-            inc=1,
-            device_id={"sp": (me + j) % n_sp},
-            device_id_type=pl.DeviceIdType.MESH,
-        )
-    pl.semaphore_wait(barrier, n_sp - 1)
-
-    down = []
-    for k in range(1, GROUPS):
-        target = ((plane + k) % GROUPS) * n_y + row
-        down.append(remote(packed_ref, packed_in.at[me], sz.at[k], rz.at[k], target))
-        down[-1].start()
-    across = []
-
-    def spread(k, source):
+    def up(k):
+        return remote(
+            packed.at[me], packed.at[me], sz.at[k], rz.at[k], at((plane + k) % GROUPS, row)
+        )
+
+    def across(k, m):
         index = ((plane + GROUPS - k) % GROUPS) * n_y + row
+        return remote(
+            packed.at[index],
+            packed.at[index],
+            sy.at[k, m],
+            ry.at[k, m],
+            at(plane, (row + m) % n_y),
+        )
+
+    raw = latent_ref[...].astype(f32)
+    scale = lax.rsqrt(jnp.mean(raw * raw, axis=-1, keepdims=True) + eps)
+    turned[...] = jnp.zeros(turned.shape, f32)
+    turned[:, :rope] = rope_ref[...].astype(f32)
+    tail = turned[...].T
+    packed[me, :tok] = (raw * scale * latent_gain_ref[...]).astype(bf)
+    packed[me, tok:, :tok] = tail[:half].astype(bf)
+    packed[me, tok:, tok : 2 * tok] = tail[half:rope].astype(bf)
+    pl.semaphore_wait(barrier, GROUPS - 1 + n_y - 1)
+    send_first = 1 + (plane + 1) // 2
+    send_last = GROUPS - 1 - 2 * (plane // 2)
+    for k in (send_first, 6 - send_first - send_last, send_last):
+
+        @pl.when(plane + k < GROUPS)
+        def _():
+            up(k).start()
+
+    for m in range(1, n_y):
+        across(0, m).start()
+
+    def positions(first, count):
+        span = pl.ds(pl.multiple_of(first * tok, tok), count)
+        return trig_ref[:half, span], trig_ref[half:, span]
+
+    cos, sin = positions(me, tok)
+    pad = 128 - qk
+    ones = jnp.ones((nope, tok), f32)
+    none = jnp.zeros((half, tok), f32)
+    empty = jnp.zeros((pad, tok), f32)
+    zeros = jnp.zeros((nope, tok), f32)
+    plain_table = jnp.concatenate([ones, cos, cos, empty], axis=0).T * gain_ref[0:1, :]
+    lower_table = jnp.concatenate([zeros, -sin, none, empty], axis=0).T * gain_ref[1:2, :]
+    upper_table = jnp.concatenate([zeros, none, sin, empty], axis=0).T * gain_ref[2:3, :]
+    lane = lax.broadcasted_iota(jnp.int32, (tok, 128), 1)
+    for h in range(heads):
+        base = h * qk // 128 * 128
+        shift = h * qk - base
+        if shift + qk <= 128:
+            x = query_ref[:, base : base + 128].astype(f32)
+            if shift:
+                x = pltpu.roll(x, 128 - shift, 1)
+        else:
+            x = query_ref[:, base : base + 256].astype(f32)
+            x = pltpu.roll(x, 256 - shift, 1)[:, :128]
+        x = jnp.where(lane < qk, x, 0.0)
+        scale = lax.rsqrt(jnp.sum(x * x, axis=-1, keepdims=True) / qk + eps)
+        y = (
+            x * plain_table
+            + pltpu.roll(x, 128 - half, 1) * lower_table
+            + pltpu.roll(x, half, 1) * upper_table
+        )
+        queries[h] = (y * scale)[:, :qk].astype(bf)
+
+    rope_low = rope_gain_ref[:half]
+    rope_high = rope_gain_ref[half:]
+
+    def attend(k, first):
+        base = (plane - k) * n_y
+        blocks = [packed[base + r] for r in range(n_y)]
+        latents = jnp.concatenate([block[:tok] for block in blocks], axis=0)
+        values[...] = dot32(latents, value_weight_ref[...]).astype(bf)
+        part = lax.dot_general(
+            key_weight_ref[...], latents, (((0,), (1,)), ((), ())), preferred_element_type=f32
+        ).astype(bf)
+        low = jnp.concatenate([block[tok:, :tok] for block in blocks], axis=1).astype(f32)
+        high = jnp.concatenate([block[tok:, tok : 2 * tok] for block in blocks], axis=1).astype(f32)
+        shared = jnp.sum(low * low + high * high, axis=0, keepdims=True)
+        cos, sin = positions(base, chunk)
+        low = low * rope_low
+        high = high * rope_high
+        rope_keys = jnp.concatenate([low * cos - high * sin, high * cos + low * sin], axis=0).astype(bf)
+        if first:
+            q_pos = row * tok + lax.broadcasted_iota(jnp.int32, (tok, chunk), 0)
+            k_pos = lax.broadcasted_iota(jnp.int32, (tok, chunk), 1)
+            allowed = k_pos // SPAN <= q_pos // SPAN
+        for h in range(heads):
+            own = part[h * nope : (h + 1) * nope]
+            square = own.astype(f32)
+            square = jnp.sum(square * square, axis=0, keepdims=True)
+            scale = lax.rsqrt((square + shared) / qk + eps) * (qk ** (-0.5) * 1.4426950408889634)
+            scores = dot32(queries[h], jnp.concatenate([own, rope_keys], axis=0)) * scale
+            if first:
+                scores = jnp.where(allowed, scores, -1e30)
+            peak = jnp.max(scores, axis=-1, keepdims=True)
+            if not first:
+                before = top[h][:, 0:1]
+                peak = jnp.maximum(before, peak)
+            raised = jnp.exp2(scores - peak).astype(bf)
+            pair = values[:, h // 2 * wide : (h // 2 + 1) * wide]
+            lanes = lax.broadcasted_iota(jnp.int32, pair.shape, 1)
+            mine = (lanes < value_width) if h % 2 == 0 else (lanes >= value_width)
+            summed = dot32(raised, jnp.where(mine, pair, jnp.ones_like(pair)))
+            if first:
+                acc[h] = summed
+            else:
+                acc[h] = acc[h] * jnp.exp2(before - peak) + summed
+            top[h] = jnp.broadcast_to(peak, top.shape[1:])
+
+    loads[0].wait()
+    loads[1].wait()
+
+    def forward(k):
+        up(k).wait_recv()
         for m in range(1, n_y):
-            target = plane * n_y + (row + m) % n_y
-            across.append(remote(source, packed_in.at[index], sy.at[k, m], ry.at[k, m], target))
-            across[-1].start()
-
-    spread(0, packed_ref)
-    sent = []
-    for j in range(1, n_sp):
-        target = (me + j) % n_sp
-        sent.append(remote(query_ref.at[target], queries_in.at[me], sq.at[j], rq.at[j], target))
-        sent[-1].start()
-    packed_in[me] = packed_ref[...]
-    queries_in[me] = query_ref[me]
-    for k in range(1, GROUPS):
-        down[k - 1].wait_recv()
-        spread(k, packed_in.at[((plane + GROUPS - k) % GROUPS) * n_y + row])
-    for copy in across:
-        copy.wait_recv()
-
-    def selector(rows, columns, source):
-        i = lax.broadcasted_iota(jnp.int32, (rows, columns), 0)
-        c = lax.broadcasted_iota(jnp.int32, (rows, columns), 1)
-        return (i == source(c)).astype(jnp.float32).astype(bf)
-
-    half = rope // 2
-
-    def swapped(c):
-        return jnp.where(c < nope, -1, jnp.where(c < nope + half, c + half, c - half))
-
-    def shape_head(plain, turned, gain, swap_gain, rows):
-        scale = lax.rsqrt(jnp.sum(plain * plain, axis=-1, keepdims=True) / qk + eps)
-        return (
-            plain * scale * gain * cos_ref[rows, :] + turned * scale * swap_gain * sin_ref[rows, :]
-        ).astype(bf)
-
-    strips = lat // rope
-    strip_rows = tok // strips
-
-    def prepare(s, carry):
-        rows = pl.ds(pl.multiple_of(s * tok, tok), tok)
-        block = packed_in[s]
-        raw = block[:tok].astype(jnp.float32)
-        scale = lax.rsqrt(jnp.mean(raw * raw, axis=-1, keepdims=True) + eps)
-        latent = (raw * scale * latent_gain_ref[...]).astype(bf)
-        values[rows, :] = dot32(latent, value_weight_ref[...]).astype(bf)
-        part = dot32(latent, key_weight_ref[...]).astype(bf)
-        tail = block[tok:]
-        plain_rope = jnp.concatenate(
-            [
-                dot32(tail, selector(lat, qk, lambda c: jnp.where(c < nope, -1, c - nope + i * rope)))
-                for i in range(strips)
-            ],
-            axis=0,
-        )
-        turned = jnp.concatenate(
-            [
-                dot32(
-                    tail,
-                    selector(
-                        lat, qk, lambda c: jnp.where(c < nope, -1, swapped(c) - nope + i * rope)
-                    ),
-                )
-                for i in range(strips)
-            ],
-            axis=0,
-        )
-        for h in range(heads):
-            plain = plain_rope + dot32(
-                part, selector(heads * nope, qk, lambda c: jnp.where(c < nope, c + h * nope, -1))
-            )
-            keys[h, rows, :] = shape_head(
-                plain, turned, key_gain_ref[...], key_swap_ref[...], rows
-            )
+            across(k, m).start()
+
+    @pl.when(plane >= 1)
+    def _():
+        forward(1)
+
+    for m in range(1, n_y):
+        across(0, m).wait_recv()
+    attend(0, True)
+
+    def later(k, carry):
+        @pl.when(plane >= k + 1)
+        def _():
+            forward(k + 1)
+
+        for m in range(1, n_y):
+            across(k, m).wait_recv()
+        attend(k, False)
         return carry
 
-    lax.fori_loop(0, n_sp, prepare, 0)
-    for copy in sent:
-        copy.wait_recv()
-
-    def prepare_queries(s, carry):
-        rows = pl.ds(pl.multiple_of(s * tok, tok), tok)
-        raw = queries_in[s]
-        for h in range(heads):
-            plain = dot32(raw, selector(heads * qk, qk, lambda c: c + h * qk))
-            turned = dot32(
-                raw,
-                selector(
-                    heads * qk, qk, lambda c: jnp.where(c < nope, -1, swapped(c) + h * qk)
-                ),
-            )
-            queries[h, rows, :] = shape_head(
-                plain, turned, query_gain_ref[...], query_swap_ref[...], rows
-            )
-        return carry
-
-    lax.fori_loop(0, n_sp, prepare_queries, 0)
-
-    blocks = 4
-    block_rows = length // blocks
-    for b in range(blocks):
-        first_row = b * block_rows
-        last_row = first_row + block_rows
-        total = None
-        lane = lax.broadcasted_iota(jnp.int32, (block_rows, heads * value_width), 1)
-        q_pos = first_row + lax.broadcasted_iota(jnp.int32, (block_rows, last_row), 0)
-        k_pos = lax.broadcasted_iota(jnp.int32, (block_rows, last_row), 1)
-        allowed = k_pos // SPAN <= q_pos // SPAN
-        for h in range(heads):
-            scores = lax.dot_general(
-                queries[h, first_row:last_row],
-                keys[h, :last_row],
-                (((1,), (1,)), ((), ())),
-                preferred_element_type=jnp.float32,
-            ) * (qk ** (-0.5))
-            scores = jnp.where(allowed, scores, -1e30)
-            raised = jnp.exp(scores - jnp.max(scores, axis=-1, keepdims=True))
-            row_sum = jnp.sum(raised, axis=-1, keepdims=True)
-            mine = dot32(raised.astype(bf), values[:last_row]) / row_sum
-            total = mine if total is None else jnp.where(lane < h * value_width, total, mine)
-        total = total.astype(bf)
-        for t in range(block_rows // tok):
-            index = first_row // tok + t
-            heads_out[index] = total[t * tok : (t + 1) * tok]
-
-            @pl.when(index != me)
-            def _():
-                remote(
-                    heads_out.at[index], token_in.at[me], so.at[index], ro.at[me], index
-                ).start()
-
-    token_in[me] = heads_out[me]
-    load.wait()
-    for j in range(1, n_sp):
-        other = (me + j) % n_sp
-        remote(
-            heads_out.at[other], token_in.at[other], so.at[other], ro.at[other], other
-        ).wait()
-    wide = heads * value_width
+    lax.fori_loop(1, plane + 1, later, 0)
+
+    lanes = lax.broadcasted_iota(jnp.int32, (tok, wide), 1)
     square = None
-    for s in range(n_sp):
-        piece = token_in[s].astype(jnp.float32)
-        part = jnp.sum(piece * piece, axis=-1, keepdims=True)
+    for p in range(heads // 2):
+        even, odd = acc[2 * p], acc[2 * p + 1]
+        total = jnp.where(lanes < value_width, odd, even)
+        out = jnp.where(lanes < value_width, even, odd) / pltpu.roll(total, value_width, 1)
+        out = out.astype(bf)
+        heads_out[:, p * wide : (p + 1) * wide] = out
+        out = out.astype(f32)
+        part = jnp.sum(out * out, axis=-1, keepdims=True)
         square = part if square is None else square + part
-    scale = lax.rsqrt(square / (n_sp * wide) + eps)
-    for s in range(n_sp):
-        span = slice(s * wide, (s + 1) * wide)
-        mixed[:, span] = (token_in[s].astype(jnp.float32) * scale * mix_gain_ref[:, span]).astype(bf)
-    stream = residual_ref[...].astype(jnp.float32) + dot32(mixed[...], out_weight_ref[...])
+    scale = lax.rsqrt(square / (heads * value_width) + eps)
+    mixed = (heads_out[...].astype(f32) * scale * mix_gain_ref[...]).astype(bf)
+    loads[2].wait()
+    stream = residual_ref[...].astype(f32) + dot32(mixed, out_weight_ref[...])
     stream_ref[...] = stream
     scale = lax.rsqrt(jnp.mean(stream * stream, axis=-1, keepdims=True) + eps)
     normed_ref[...] = (stream * scale * ffn_gain_ref[...]).astype(bf)
-    for copy in down + across + sent:
-        copy.wait_send()
+    for m in range(1, n_y):
+        across(0, m).wait_send()
+    for k in range(1, GROUPS):
+
+        @pl.when(plane + k < GROUPS)
+        def _():
+            up(k).wait_send()
+
+        @pl.when(plane >= k)
+        def _():
+            for m in range(1, n_y):
+                across(k, m).wait_send()
 
 
 def attended(
@@ -504,78 +525,69 @@
 ):
     n_sp = lax.axis_size("sp")
     n_y = n_sp // GROUPS
-    me = lax.axis_index("sp")
     tok, width = residual.shape
     rope = rope_key.shape[1]
     qk = nope + rope
     lat = latent.shape[1]
-    heads = head_count // n_sp
-    length = n_sp * tok
     half = rope // 2
     bf = jnp.bfloat16
-    query_blocks = query.reshape(tok, n_sp, heads * qk).transpose(1, 0, 2)
-    strips = lat // rope
-    tail = rope_key.reshape(strips, tok // strips, rope).transpose(1, 0, 2).reshape(-1, lat)
-    packed = jnp.concatenate([latent, tail], axis=0)
-    phases = angles(0, length, rope)
-    cos, sin = jnp.cos(phases), jnp.sin(phases)
-    cos = jnp.concatenate([jnp.ones((length, nope), jnp.float32), cos, cos], axis=1)
-    sin = jnp.concatenate([jnp.zeros((length, nope), jnp.float32), -sin, sin], axis=1)
-
-    def swap(gain):
-        return jnp.concatenate([gain[:nope], gain[nope + half :], gain[nope : nope + half]])
-
-    key_own = lax.dynamic_slice_in_dim(key_weight, me * heads * nope, heads * nope, 1)
-    value_own = lax.dynamic_slice_in_dim(value_weight, me * heads * value_width, heads * value_width, 1)
+    phases = angles(0, n_sp * tok, rope).T
+    trig = jnp.concatenate([jnp.cos(phases), jnp.sin(phases)], axis=0)
+    zero = jnp.zeros((128 - qk,), jnp.float32)
+    blank = jnp.zeros((nope,), jnp.float32)
+    gap = jnp.zeros((half,), jnp.float32)
+    own = query_gain * jnp.concatenate([key_gain[:nope], jnp.ones((rope,), jnp.float32)])
+    gains = jnp.stack(
+        [
+            jnp.concatenate([own, zero]),
+            jnp.concatenate([blank, query_gain[nope + half :], gap, zero]),
+            jnp.concatenate([blank, gap, query_gain[nope : nope + half], zero]),
+        ]
+    )
     vmem = pl.BlockSpec(memory_space=pltpu.VMEM)
+    hbm = pl.BlockSpec(memory_space=pl.ANY)
     dma = pltpu.SemaphoreType.DMA
-    wide = heads * value_width
     return pl.pallas_call(
-        functools.partial(attention_kernel, n_sp, n_y, heads, nope, rope, value_width),
+        functools.partial(attention_kernel, n_sp, n_y, head_count, nope, rope, value_width),
         out_shape=(
             jax.ShapeDtypeStruct((tok, width), jnp.float32),
             jax.ShapeDtypeStruct((tok, width), bf),
         ),
-        in_specs=[vmem] * 14 + [pl.BlockSpec(memory_space=pl.ANY)],
+        in_specs=[vmem] * 10 + [hbm] * 3,
         out_specs=(vmem, vmem),
         scratch_shapes=[
+            pltpu.VMEM(key_weight.shape, bf),
+            pltpu.VMEM(value_weight.shape, bf),
             pltpu.VMEM(out_weight.shape, bf),
-            pltpu.VMEM((n_sp, tok, heads * qk), bf),
-            pltpu.VMEM((n_sp,) + packed.shape, bf),
-            pltpu.VMEM((heads, length, qk), bf),
-            pltpu.VMEM((heads, length, qk), bf),
-            pltpu.VMEM((length, wide), bf),
-            pltpu.VMEM((n_sp, tok, wide), bf),
-            pltpu.VMEM((n_sp, tok, wide), bf),
-            pltpu.VMEM((tok, n_sp * wide), bf),
-            dma((1,)),
-            dma((n_sp,)),
-            dma((n_sp,)),
+            pltpu.VMEM((tok, 128), jnp.float32),
+            pltpu.VMEM((n_sp, tok + half, lat), bf),
+            pltpu.VMEM((head_count, tok, qk), bf),
+            pltpu.VMEM((n_y * tok, head_count * value_width), bf),
+            pltpu.VMEM((head_count, tok, 128), jnp.float32),
+            pltpu.VMEM((head_count, tok, 2 * value_width), jnp.float32),
+            pltpu.VMEM((tok, head_count * value_width), bf),
+            dma((3,)),
             dma((GROUPS,)),
             dma((GROUPS,)),
             dma((GROUPS, n_y)),
             dma((GROUPS, n_y)),
-            dma((n_sp,)),
-            dma((n_sp,)),
         ],
         compiler_params=pltpu.CompilerParams(
             collective_id=1, has_side_effects=True, vmem_limit_bytes=48 * 1024 * 1024
         ),
     )(
-        query_blocks,
-        packed,
+        query,
+        latent,
+        rope_key,
         latent_gain[None],
-        query_gain[None],
-        swap(query_gain)[None],
-        key_gain[None],
-        swap(key_gain)[None],
-        cos,
-        sin,
-        key_own,
-        value_own,
+        gains,
+        key_gain[nope:, None],
+        trig,
         residual,
         mix_gain[None],
         ffn_gain[None],
+        key_weight,
+        value_weight,
         out_weight,
     )
 

time: 132 us -> 110 us (0.83)
  Pallas kernels: 120 us -> 93.1 us
  local copies, waits for them, and re-layouts: 6.77 us -> 12.7 us
    pallas_call x1, Pallas kernels: 35.4 us -> 13.1 us  [attended(): pl.pallas_call(functools.partial(attention_kernel, n_sp, n_y, head_count,...]
    unnamed x33 -> x24, local copies, waits for them, and re-layouts: 4.28 us -> 9.95 us
    pallas_call x1, Pallas kernels: 85 us -> 80 us  [routed(): pl.pallas_call(functools.partial(expert_kernel, n_y, n_dp, cap, rows), ou...]
    neg x1 -> x0, other arithmetic: 1.9 us -> none  [attended(): -sin]
where the time goes in v2:
time: 110 us
  Pallas kernels  93.1 us (85%)
  local copies, waits for them, and re-layouts  12.7 us (12%)
  other arithmetic  4.1 us (4%)
    pallas_call x1, Pallas kernels, routed(): pl.pallas_call(functools.partial(expert_kernel, n_y, n_dp, cap, rows), ou...  80 us
    pallas_call x1, Pallas kernels, attended(): pl.pallas_call(functools.partial(attention_kernel, n_sp, n_y, head_count,...  13.1 us
    unnamed x24, local copies, waits for them, and re-layouts  9.95 us

profile of v2, /device:TPU:0, one launch (start us, length us, event | category | flops | bytes accessed | tf_op | source)
XLA Modules:
  0.0 110.0 jit_solution(4013097314341232754)
XLA Ops:
  0.0 0.0 copy-start.3
  0.0 0.0 copy-start.2
  0.0 0.0 copy-start.1
  0.0 0.8 select_multiply_fusion
  0.8 0.7 slice_bitcast_fusion
  1.5 0.7 reduce_sum.28
  2.3 0.8 fusion.11
  3.1 0.1 fusion.6
  3.2 0.1 copy.36.rope_gain_ref
  3.3 0.8 copy.35
  4.1 0.8 copy.37
  4.9 0.1 copy.39
  4.9 0.2 convert_reduce_fusion
  5.2 0.2 fusion.8
  5.3 0.1 subtract_multiply_fusion
  5.4 0.1 copy.41
  5.5 0.2 convert_reduce_fusion.1
  5.7 0.1 copy.43
  5.9 0.7 compare_convert_fusion.pick_ref
  6.6 0.8 copy.42
  7.4 0.8 fusion
  8.1 0.1 fusion.9
  8.2 0.7 concatenate.24.info_ref
  9.0 0.3 multiply_cosine_fusion
  9.3 0.0 copy-done.3
  9.3 0.0 copy-done.2
  9.3 0.0 copy-done.1
  9.3 0.0 copy-start.5
  9.3 1.0 copy-done.5
  10.3 0.0 copy-start.6
  10.3 0.8 copy-done.6
  11.2 0.0 copy-start.7
  11.2 0.7 copy-done.7
  11.9 0.0 copy-start.8
  11.9 0.7 copy-done.8
  12.6 0.0 copy-start.9
  12.6 0.7 copy-done.9
  13.2 13.1 %shard_map.172 = (f32[128,2048]{1,0:T(8,128)S(1)}, bf16[128,2048]{1,0:T(8,128)(2,1)S(1)}) custom-call(bf16[128,1536]{1,0:T(8,128)(2,1)S(1)} %bitcast.31, bf16[128,256]{1,0:T(8,128)(2,1)S(1)} %bitcast.33, bf16[128,32]{1,0:T(8,128)(2,1)S(1)} %bitcast.32, f32[1,256]{1,0:T(1,128)S(1)} %bitcast.36, f32[3,128]{1,0:T(4,128)S(1)} %pad_maximum_fusion.1.gain_ref, ...), custom_call_target="tpu_custom_call" | custom-call | tf_op jit(solution)/shard_map/pallas_call | solution.py:550
  26.3 0.0 copy-start
  26.3 1.0 copy-done
  27.3 0.0 copy-start.4
  27.3 0.8 copy-done.4
  28.1 80.0 %shard_map.173 = bf16[128,2048]{1,0:T(8,128)(2,1)} custom-call(bf16[128,2048]{1,0:T(8,128)(2,1)} %copy-done.4, bf16[128,128]{1,0:T(8,128)(2,1)} %concatenate.24.info_ref, bf16[4,64,128]{2,1,0:T(8,128)(2,1)} %compare_convert_fusion.pick_ref, f32[128,2048]{1,0:T(8,128)} %copy-done, bf16[2048,512]{1,0:T(8,128)(2,1)} %bitcast.38, bf16[2048,512]{1,0:T(8,128)(2,1)} %bitcast.39, ...), custom_call_target="tpu_custom_call" | custom-call | tf_op jit(solution)/shard_map/pallas_call | solution.py:637
  108.1 1.9 %copy.45 = bf16[1,128,2048]{2,1,0:T(8,128)(2,1)} copy(bf16[1,128,2048]{2,1,0:T(8,128)(2,1)} %bitcast.37) | data formatting | bytes 1048576
  (13 shorter events, 0.1 us)
Async XLA Ops:
  0.0 9.3 %copy-start.3 = (bf16[256,1024]{1,0:T(8,128)(2,1)S(1)}, bf16[256,1024]{1,0:T(8,128)(2,1)}, u32[]{:S(2)}) copy-start(bf16[256,1024]{1,0:T(8,128)(2,1)} %value_weight_hbm.1) | copy-start | bytes 1572868
  0.0 9.3 %copy-start.2 = (bf16[256,1024]{1,0:T(8,128)(2,1)S(1)}, bf16[256,1024]{1,0:T(8,128)(2,1)}, u32[]{:S(2)}) copy-start(bf16[256,1024]{1,0:T(8,128)(2,1)} %key_weight_hbm.1) | copy-start | bytes 1572868
  0.0 9.3 %copy-start.1 = (bf16[1,128,2048]{2,1,0:T(8,128)(2,1)S(1)}, bf16[1,128,2048]{2,1,0:T(8,128)(2,1)}, u32[]{:S(2)}) copy-start(bf16[1,128,2048]{2,1,0:T(8,128)(2,1)} %param.18) | copy-start | bytes 1572868
  9.3 1.0 copy-start.5
  10.3 0.8 copy-start.6
  11.2 0.7 copy-start.7
  11.9 0.7 copy-start.8
  12.6 0.7 copy-start.9
  26.3 1.0 copy-start
  27.3 0.8 copy-start.4

commit v3 on v2

v3 whole, which is shorter than its diff:
```python
import functools

import jax
import jax.numpy as jnp
from jax import lax
from jax.experimental import pallas as pl
from jax.experimental.pallas import tpu as pltpu
from jax.sharding import PartitionSpec as P

GROUPS = 4
SPAN = 64


eps = 1e-06


def angles(offset, span_count, rope_width):
    position = (offset + jnp.arange(span_count, dtype=jnp.int32)).astype(jnp.float32)
    frequency = 10000.0 ** (-2.0 * jnp.arange(rope_width // 2, dtype=jnp.float32) / rope_width)
    return position[:, None] * frequency[None, :]


def dot32(a, b):
    return jnp.dot(a, b, preferred_element_type=jnp.float32)


def dot_t(a, b):
    return lax.dot_general(a, b, (((0,), (0,)), ((), ())), preferred_element_type=jnp.float32)


def layer_kernel(
    n_sp,
    n_y,
    n_dp,
    heads,
    nope,
    rope,
    value_width,
    cap,
    rows,
    residual_hbm,
    query_hbm,
    latent_hbm,
    rope_hbm,
    latent_gain_hbm,
    query_gain_hbm,
    key_gain_hbm,
    cos_hbm,
    sin_hbm,
    mix_gain_hbm,
    ffn_gain_hbm,
    choice_hbm,
    group_prob_hbm,
    share_hbm,
    key_weight_hbm,
    value_weight_hbm,
    out_weight_hbm,
    gate_hbm,
    up_hbm,
    down_hbm,
    out_ref,
    residual_ref,
    query_ref,
    latent_ref,
    rope_ref,
    latent_gain_ref,
    query_gain_ref,
    key_gain_ref,
    cos_ref,
    sin_ref,
    mix_gain_ref,
    ffn_gain_ref,
    choice_ref,
    group_prob_ref,
    share_ref,
    key_weight_ref,
    value_weight_ref,
    out_weight_ref,
    gate_ref,
    up_ref,
    down_ref,
    gains,
    packed,
    queries,
    values,
    top,
    acc,
    heads_out,
    stream_ref,
    normed_ref,
    picks,
    notes_out,
    notes,
    out1,
    in1,
    out2,
    arrive,
    served,
    back2,
    merged,
    home,
    w_sem,
    sz,
    rz,
    sy,
    ry,
    s0,
    r0,
    s1,
    r1,
    s2,
    r2,
    s3,
    r3,
    s4,
    r4,
):
    bf = jnp.bfloat16
    f32 = jnp.float32
    tok = latent_ref.shape[0]
    qk = nope + rope
    half = rope // 2
    wide = 2 * value_width
    chunk = n_y * tok
    peers = n_y * n_dp
    chunks = in1.shape[1]
    part = in1.shape[3]
    me = lax.axis_index("sp")
    dp = lax.axis_index("dp")
    plane = me // n_y
    row = me % n_y
    mine = row * n_dp + dp

    def column(k):
        return {"sp": ((plane + k) % GROUPS) * n_y + row, "dp": dp}

    def peer(j):
        other = (mine + j) % peers
        return {"sp": plane * n_y + other // n_dp, "dp": other % n_dp}

    def at(index_plane, index_row):
        return {"sp": index_plane * n_y + index_row}

    barrier = pltpu.get_barrier_semaphore()
    for k in range(1, GROUPS):
        pl.semaphore_signal(barrier, inc=1, device_id=column(k), device_id_type=pl.DeviceIdType.MESH)
    for j in range(1, peers):
        pl.semaphore_signal(barrier, inc=1, device_id=peer(j), device_id_type=pl.DeviceIdType.MESH)

    pairs = (
        (latent_hbm, latent_ref),
        (latent_gain_hbm, latent_gain_ref),
        (rope_hbm, rope_ref),
        (choice_hbm, choice_ref),
        (group_prob_hbm, group_prob_ref),
        (share_hbm, share_ref),
        (query_gain_hbm, query_gain_ref),
        (key_gain_hbm, key_gain_ref),
        (cos_hbm, cos_ref),
        (sin_hbm, sin_ref),
        (query_hbm, query_ref),
        (key_weight_hbm, key_weight_ref),
        (value_weight_hbm, value_weight_ref),
        (residual_hbm, residual_ref),
        (mix_gain_hbm, mix_gain_ref),
        (ffn_gain_hbm, ffn_gain_ref),
        (out_weight_hbm, out_weight_ref),
        (gate_hbm, gate_ref),
        (up_hbm, up_ref),
        (down_hbm, down_ref),
    )
    copies = [
        (source, pltpu.make_async_copy(source, target, w_sem.at[i]))
        for i, (source, target) in enumerate(pairs)
    ]
    for _, copy in copies:
        copy.start()

    def ready(*sources):
        for source, copy in copies:
            if any(source is wanted for wanted in sources):
                copy.wait()

    def remote(src, dst, send, recv, target):
        return pltpu.make_async_remote_copy(
            src_ref=src,
            dst_ref=dst,
            send_sem=send,
            recv_sem=recv,
            device_id=target,
            device_id_type=pl.DeviceIdType.MESH,
        )

    def up(k):
        return remote(
            packed.at[me], packed.at[me], sz.at[k], rz.at[k], at((plane + k) % GROUPS, row)
        )

    def across(k, m):
        index = ((plane + GROUPS - k) % GROUPS) * n_y + row
        return remote(
            packed.at[index],
            packed.at[index],
            sy.at[k, m],
            ry.at[k, m],
            at(plane, (row + m) % n_y),
        )

    send_first = 1 + (plane + 1) // 2
    send_last = GROUPS - 1 - 2 * (plane // 2)
    send_order = (send_first, 6 - send_first - send_last, send_last)
    recv_first = 6 - send_first - send_last
    recv_last = 1 + 2 * (plane % 2)
    recv_order = (recv_first, 6 - recv_first - recv_last, recv_last)

    def span(c):
        return slice(c * part, (c + 1) * part)

    def note(k):
        return remote(notes_out.at[k], notes.at[k], s0.at[k], r0.at[k], column(k))

    def first(k, c):
        return remote(out1.at[k, c], in1.at[k, c], s1.at[k, c], r1.at[k, c], column(k))

    def second(k, c, j):
        return remote(
            out2.at[k, c, (mine + j) % peers],
            arrive.at[k, c, j],
            s2.at[k, c, j],
            r2.at[k, c, j],
            peer(j),
        )

    def third(k, c, j):
        return remote(
            served.at[k, c, j],
            back2.at[k, c, mine],
            s3.at[k, c, j],
            r3.at[k, c, peers - j],
            peer(peers - j),
        )

    def fourth(k, c):
        return remote(merged.at[k, c], home.at[k, c], s4.at[k, c], r4.at[k, c], column(GROUPS - k))

    ready(latent_hbm, latent_gain_hbm, rope_hbm)
    raw = latent_ref[...].astype(f32)
    scale = lax.rsqrt(jnp.mean(raw * raw, axis=-1, keepdims=True) + eps)
    packed[me, :tok] = (raw * scale * latent_gain_ref[...]).astype(bf)
    packed[me, tok:, :tok] = rope_ref[:half]
    packed[me, tok:, tok : 2 * tok] = rope_ref[half:]
    pl.semaphore_wait(barrier, GROUPS - 1 + peers - 1)
    for k in send_order:

        @pl.when(plane + k < GROUPS)
        def _():
            up(k).start()

    for m in range(1, n_y):
        across(0, m).start()

    def positions(first, count):
        span = pl.ds(pl.multiple_of(first * tok, tok), count)
        return cos_ref[:, span], sin_ref[:, span]

    ready(query_gain_hbm, key_gain_hbm, cos_hbm, sin_hbm)
    gains[...] = jnp.zeros(gains.shape, f32)
    gains[0:1, :qk] = query_gain_ref[...]
    gains[1:2, :qk] = key_gain_ref[...]
    both = gains[...]
    lane = lax.broadcasted_iota(jnp.int32, (1, 128), 1)
    plain_gain = both[0:1] * jnp.where(lane < nope, both[1:2], 1.0)
    lower_gain = pltpu.roll(both, 128 - half, 1)[0:1]
    upper_gain = pltpu.roll(both, half, 1)[0:1]
    key_gains = jnp.broadcast_to(both[1:2], (128, 128)).T
    rope_low = key_gains[nope : nope + half, 0:1]
    rope_high = key_gains[nope + half : qk, 0:1]
    ready(query_hbm)
    cos, sin = positions(me, tok)
    pad = 128 - qk
    ones = jnp.ones((nope, tok), f32)
    none = jnp.zeros((half, tok), f32)
    empty = jnp.zeros((pad, tok), f32)
    zeros = jnp.zeros((nope, tok), f32)
    plain_table = jnp.concatenate([ones, cos, cos, empty], axis=0).T * plain_gain
    lower_table = jnp.concatenate([zeros, -sin, none, empty], axis=0).T * lower_gain
    upper_table = jnp.concatenate([zeros, none, sin, empty], axis=0).T * upper_gain
    lane = lax.broadcasted_iota(jnp.int32, (tok, 128), 1)
    for h in range(heads):
        base = h * qk // 128 * 128
        shift = h * qk - base
        if shift + qk <= 128:
            x = query_ref[:, base : base + 128].astype(f32)
            if shift:
                x = pltpu.roll(x, 128 - shift, 1)
        else:
            x = query_ref[:, base : base + 256].astype(f32)
            x = pltpu.roll(x, 256 - shift, 1)[:, :128]
        x = jnp.where(lane < qk, x, 0.0)
        scale = lax.rsqrt(jnp.sum(x * x, axis=-1, keepdims=True) / qk + eps)
        y = (
            x * plain_table
            + pltpu.roll(x, 128 - half, 1) * lower_table
            + pltpu.roll(x, half, 1) * upper_table
        )
        queries[h] = (y * scale)[:, :qk].astype(bf)


    ready(choice_hbm, group_prob_hbm, share_hbm)
    per_group = peers
    group = choice_ref[0:1] // per_group
    order = lax.broadcasted_iota(jnp.int32, (tok, tok), 0)
    sooner = order < lax.broadcasted_iota(jnp.int32, (tok, tok), 1)

    def tall(line):
        return jnp.broadcast_to(line.astype(f32), (tok, tok)).T

    def count(flags):
        return jnp.sum(jnp.where(sooner & flags, 1.0, 0.0), axis=0, keepdims=True)

    rank = count(tall(group) == group.astype(f32))
    line = group.astype(f32) * rows + rank
    for g in range(GROUPS):
        slot = g * rows + lax.broadcasted_iota(jnp.int32, (rows, tok), 0)
        picks[g] = jnp.where(slot.astype(f32) == line, 1.0, 0.0).astype(bf)
    talls = (tall(choice_ref[0:1]), tall(choice_ref[1:2]))
    facts = []
    for s in range(2):
        named = choice_ref[s : s + 1].astype(f32)
        earlier = count(talls[0] == named) + count(talls[1] == named)
        facts.append((named - group.astype(f32) * per_group) * cap + earlier)
    total = share_ref[0:1] + share_ref[1:2]
    for s in range(2):
        route = group_prob_ref[...] * share_ref[s : s + 1] / total
        high = route.astype(bf).astype(f32)
        facts.append(high)
        facts.append(route - high)
    facts.append(jnp.zeros((128 - len(facts), tok), f32))
    facts = jnp.concatenate(facts, axis=0).astype(bf)

    def describe(g):
        return lax.dot_general(
            picks[g], facts, (((1,), (1,)), ((), ())), preferred_element_type=f32
        ).astype(bf)

    notes[0] = describe(plane)
    for k in send_order:
        notes_out[k] = describe((plane + k) % GROUPS)
        note(k).start()

    def attend(k, first):
        base = (plane - k) * n_y
        blocks = [packed[base + r] for r in range(n_y)]
        latents = jnp.concatenate([block[:tok] for block in blocks], axis=0)
        values[...] = dot32(latents, value_weight_ref[...]).astype(bf)
        part = lax.dot_general(
            key_weight_ref[...], latents, (((0,), (1,)), ((), ())), preferred_element_type=f32
        ).astype(bf)
        low = jnp.concatenate([block[tok:, :tok] for block in blocks], axis=1).astype(f32)
        high = jnp.concatenate([block[tok:, tok : 2 * tok] for block in blocks], axis=1).astype(f32)
        shared = jnp.sum(low * low + high * high, axis=0, keepdims=True)
        cos, sin = positions(base, chunk)
        low = low * rope_low
        high = high * rope_high
        rope_keys = jnp.concatenate([low * cos - high * sin, high * cos + low * sin], axis=0).astype(bf)
        if first:
            q_pos = row * tok + lax.broadcasted_iota(jnp.int32, (tok, chunk), 0)
            k_pos = lax.broadcasted_iota(jnp.int32, (tok, chunk), 1)
            allowed = k_pos // SPAN <= q_pos // SPAN
        for h in range(heads):
            own = part[h * nope : (h + 1) * nope]
            square = own.astype(f32)
            square = jnp.sum(square * square, axis=0, keepdims=True)
            scale = lax.rsqrt((square + shared) / qk + eps) * (qk ** (-0.5) * 1.4426950408889634)
            scores = dot32(queries[h], jnp.concatenate([own, rope_keys], axis=0)) * scale
            if first:
                scores = jnp.where(allowed, scores, -1e30)
            peak = jnp.max(scores, axis=-1, keepdims=True)
            if not first:
                before = top[h][:, 0:1]
                peak = jnp.maximum(before, peak)
            raised = jnp.exp2(scores - peak).astype(bf)
            pair = values[:, h // 2 * wide : (h // 2 + 1) * wide]
            lanes = lax.broadcasted_iota(jnp.int32, pair.shape, 1)
            mine = (lanes < value_width) if h % 2 == 0 else (lanes >= value_width)
            summed = dot32(raised, jnp.where(mine, pair, jnp.ones_like(pair)))
            if first:
                acc[h] = summed
            else:
                acc[h] = acc[h] * jnp.exp2(before - peak) + summed
            top[h] = jnp.broadcast_to(peak, top.shape[1:])

    ready(key_weight_hbm, value_weight_hbm)

    def forward(k):
        up(k).wait_recv()
        for m in range(1, n_y):
            across(k, m).start()

    @pl.when(plane >= 1)
    def _():
        forward(1)

    for m in range(1, n_y):
        across(0, m).wait_recv()
    attend(0, True)

    def later(k, carry):
        @pl.when(plane >= k + 1)
        def _():
            forward(k + 1)

        for m in range(1, n_y):
            across(k, m).wait_recv()
        attend(k, False)
        return carry

    lax.fori_loop(1, plane + 1, later, 0)

    lanes = lax.broadcasted_iota(jnp.int32, (tok, wide), 1)
    square = None
    for p in range(heads // 2):
        even, odd = acc[2 * p], acc[2 * p + 1]
        total = jnp.where(lanes < value_width, odd, even)
        out = jnp.where(lanes < value_width, even, odd) / pltpu.roll(total, value_width, 1)
        out = out.astype(bf)
        heads_out[:, p * wide : (p + 1) * wide] = out
        out = out.astype(f32)
        term = jnp.sum(out * out, axis=-1, keepdims=True)
        square = term if square is None else square + term
    scale = lax.rsqrt(square / (heads * value_width) + eps)
    ready(mix_gain_hbm)
    mixed = (heads_out[...].astype(f32) * scale * mix_gain_ref[...]).astype(bf)
    ready(residual_hbm, ffn_gain_hbm, out_weight_hbm)
    stream = residual_ref[...].astype(f32) + dot32(mixed, out_weight_ref[...])
    stream_ref[...] = stream
    scale = lax.rsqrt(jnp.mean(stream * stream, axis=-1, keepdims=True) + eps)
    normed_ref[...] = (stream * scale * ffn_gain_ref[...]).astype(bf)
    for k in send_order:
        chosen = picks[(plane + k) % GROUPS]
        for c in range(chunks):
            out1[k, c] = dot32(chosen, normed_ref[:, span(c)]).astype(bf)
            first(k, c).start()
    own = picks[plane]
    for c in range(chunks):
        in1[0, c] = dot32(own, normed_ref[:, span(c)]).astype(bf)

    def slots(k):
        info = notes[k].astype(jnp.float32)
        place = lax.broadcasted_iota(jnp.int32, (rows, peers * cap), 1).astype(jnp.float32)
        return place == info[:, 0:1], place == info[:, 1:2], info

    def scatter(k, local):
        if not local:
            note(k).wait_recv()
        at0, at1, _ = slots(k)
        choose = (at0.astype(jnp.float32) + at1.astype(jnp.float32)).astype(bf)
        for c in range(chunks):
            if not local:
                first(k, c).wait_recv()
            placed = dot_t(choose, in1[k, c]).astype(bf)
            for e in range(peers):
                out2[k, c, e] = placed[e * cap : (e + 1) * cap]
            for j in range(1, peers):
                second(k, c, j).start()
            arrive[k, c, 0] = out2[k, c, mine]

    def serve(k, load):
        gate_act = None
        for c in range(chunks):
            for j in range(1, peers):
                second(k, c, j).wait_recv()
            if load and c == 0:
                ready(gate_hbm, up_hbm, down_hbm)
            given = arrive[k, c].reshape(peers * cap, part)
            gate_part = dot32(given, gate_ref[span(c), :])
            up_part = dot32(given, up_ref[span(c), :])
            gate_act = gate_part if gate_act is None else gate_act + gate_part
            upward = up_part if c == 0 else upward + up_part
        hidden = (gate_act * (1.0 / (1.0 + jnp.exp(-gate_act))) * upward).astype(bf)
        for c in range(chunks):
            result = dot32(hidden, down_ref[:, span(c)]).astype(bf)
            for j in range(peers):
                served[k, c, j] = result[j * cap : (j + 1) * cap]
            for j in range(1, peers):
                third(k, c, j).start()
            back2[k, c, mine] = served[k, c, 0]

    def merge(k, local):
        at0, at1, info = slots(k)
        high = jnp.where(at0, info[:, 2:3], 0.0) + jnp.where(at1, info[:, 4:5], 0.0)
        low = jnp.where(at0, info[:, 3:4], 0.0) + jnp.where(at1, info[:, 5:6], 0.0)
        high = high.astype(bf)
        low = low.astype(bf)
        for c in range(chunks):
            for j in range(1, peers):
                third(k, c, j).wait_recv()
            got = back2[k, c].reshape(peers * cap, part)
            total = (dot32(high, got) + dot32(low, got)).astype(bf)
            if local:
                home[0, c] = total
            else:
                merged[k, c] = total
                fourth(k, c).start()

    scatter(0, True)
    scatter(recv_order[0], False)
    scatter(recv_order[1], False)
    serve(recv_order[0], True)
    serve(recv_order[1], False)
    merge(recv_order[0], False)
    scatter(recv_order[2], False)
    merge(recv_order[1], False)
    serve(recv_order[2], False)
    serve(0, False)
    merge(recv_order[2], False)
    merge(0, True)
    for c in range(chunks):
        total = stream_ref[:, span(c)] + dot_t(own, home[0, c])
        for k in send_order:
            fourth(k, c).wait_recv()
            total = total + dot_t(picks[(plane + k) % GROUPS], home[k, c])
        out_ref[:, span(c)] = total.astype(bf)
    for k in range(GROUPS):
        if k:
            note(k).wait_send()
        for c in range(chunks):
            if k:
                first(k, c).wait_send()
                fourth(k, c).wait_send()
            for j in range(1, peers):
                second(k, c, j).wait_send()
                third(k, c, j).wait_send()
    for m in range(1, n_y):
        across(0, m).wait_send()
    for k in range(1, GROUPS):

        @pl.when(plane + k < GROUPS)
        def _():
            up(k).wait_send()

        @pl.when(plane >= k)
        def _():
            for m in range(1, n_y):
                across(k, m).wait_send()


def per_device(
    residual,
    query,
    latent,
    rope_key,
    latent_gain,
    query_gain,
    key_gain,
    key_weight,
    value_weight,
    mix_gain,
    out_weight,
    ffn_gain,
    expert_choice,
    group_prob,
    expert_prob,
    gate_weight,
    up_weight,
    down_weight,
):
    n_sp = lax.axis_size("sp")
    n_dp = lax.axis_size("dp")
    n_y = n_sp // GROUPS
    _, tok, width = residual.shape
    rope = rope_key.shape[2]
    qk = query_gain.shape[0]
    nope = qk - rope
    heads = query.shape[2] // qk
    value_width = value_weight.shape[1] // heads
    lat = latent.shape[2]
    hidden = gate_weight.shape[2]
    experts = n_sp * n_dp
    peers = experts // GROUPS
    cap = tok * GROUPS // experts
    rows = peers * cap // expert_choice.shape[2]
    chunks = 4
    part = width // chunks
    bf = jnp.bfloat16
    f32 = jnp.float32
    phases = angles(0, n_sp * tok, rope).T
    operands = (
        residual[0],
        query[0],
        latent[0],
        rope_key[0].T,
        latent_gain[None],
        query_gain[None],
        key_gain[None],
        jnp.cos(phases),
        jnp.sin(phases),
        mix_gain[None],
        ffn_gain[None],
        expert_choice[0].T,
        group_prob,
        expert_prob[0].T,
        key_weight,
        value_weight,
        out_weight,
        gate_weight[0],
        up_weight[0],
        down_weight[0],
    )
    vmem = pl.BlockSpec(memory_space=pltpu.VMEM)
    hbm = pl.BlockSpec(memory_space=pl.ANY)
    dma = pltpu.SemaphoreType.DMA
    return pl.pallas_call(
        functools.partial(layer_kernel, n_sp, n_y, n_dp, heads, nope, rope, value_width, cap, rows),
        out_shape=jax.ShapeDtypeStruct((tok, width), bf),
        in_specs=[hbm] * len(operands),
        out_specs=vmem,
        scratch_shapes=[pltpu.VMEM(a.shape, a.dtype) for a in operands]
        + [
            pltpu.VMEM((8, 128), f32),
            pltpu.VMEM((n_sp, tok + rope // 2, lat), bf),
            pltpu.VMEM((heads, tok, qk), bf),
            pltpu.VMEM((n_y * tok, heads * value_width), bf),
            pltpu.VMEM((heads, tok, 128), f32),
            pltpu.VMEM((heads, tok, 2 * value_width), f32),
            pltpu.VMEM((tok, heads * value_width), bf),
            pltpu.VMEM((tok, width), f32),
            pltpu.VMEM((tok, width), bf),
            pltpu.VMEM((GROUPS, rows, tok), bf),
            pltpu.VMEM((GROUPS, rows, 128), bf),
            pltpu.VMEM((GROUPS, rows, 128), bf),
            pltpu.VMEM((GROUPS, chunks, rows, part), bf),
            pltpu.VMEM((GROUPS, chunks, rows, part), bf),
            pltpu.VMEM((GROUPS, chunks, peers, cap, part), bf),
            pltpu.VMEM((GROUPS, chunks, peers, cap, part), bf),
            pltpu.VMEM((GROUPS, chunks, peers, cap, part), bf),
            pltpu.VMEM((GROUPS, chunks, peers, cap, part), bf),
            pltpu.VMEM((GROUPS, chunks, rows, part), bf),
            pltpu.VMEM((GROUPS, chunks, rows, part), bf),
            dma((len(operands),)),
            dma((GROUPS,)),
            dma((GROUPS,)),
            dma((GROUPS, n_y)),
            dma((GROUPS, n_y)),
            dma((GROUPS,)),
            dma((GROUPS,)),
            dma((GROUPS, chunks)),
            dma((GROUPS, chunks)),
            dma((GROUPS, chunks, peers)),
            dma((GROUPS, chunks, peers)),
            dma((GROUPS, chunks, peers)),
            dma((GROUPS, chunks, peers)),
            dma((GROUPS, chunks)),
            dma((GROUPS, chunks)),
        ],
        compiler_params=pltpu.CompilerParams(
            collective_id=0, has_side_effects=True, vmem_limit_bytes=60 * 1024 * 1024
        ),
    )(*operands)[None]


def solution(mesh):
    return jax.shard_map(
        per_device,
        mesh=mesh,
        in_specs=(
            P("dp", "sp", None),
            P("dp", "sp", None),
            P("dp", "sp", None),
            P("dp", "sp", None),
            P(),
            P(),
            P(),
            P(),
            P(),
            P(),
            P(),
            P(),
            P("dp", "sp", None),
            P("dp", "sp"),
            P("dp", "sp", None),
            P(("sp", "dp"), None, None),
            P(("sp", "dp"), None, None),
            P(("sp", "dp"), None, None),
        ),
        out_specs=P("dp", "sp", None),
        check_vma=False,
    )
```

time: 110 us -> 92.4 us (0.84)
  local copies, waits for them, and re-layouts: 12.7 us -> 1.88 us
  Pallas kernels: 93.1 us -> 89.4 us
  other arithmetic: 4.1 us -> 0.99 us
    unnamed x24 -> x1, local copies, waits for them, and re-layouts: 9.95 us -> 1.88 us
    pallas_call x2 -> x1, Pallas kernels: 93.1 us -> 89.4 us  [per_device(): pl.pallas_call(functools.partial(layer_kernel, n_sp, n_y, n_dp, heads, no...]
where the time goes in v3:
time: 92.4 us; the launch traced here: 92.2 us
  Pallas kernels  89.4 us (97%)
  local copies, waits for them, and re-layouts  1.88 us (2%)
  other arithmetic  0.99 us (1%)
    pallas_call x1, Pallas kernels, per_device(): pl.pallas_call(functools.partial(layer_kernel, n_sp, n_y, n_dp, heads, no...  89.4 us
    unnamed x1, local copies, waits for them, and re-layouts  1.88 us

profile of v3, /device:TPU:0, one launch (start us, length us, event | category | flops | bytes accessed | tf_op | source)
XLA Modules:
  0.0 92.2 jit_solution(6110341758336037599)
XLA Ops:
  0.0 1.0 %multiply_sine_fusion = (f32[16,1024]{1,0:T(8,128)}, f32[16,1024]{1,0:T(8,128)}) fusion(f32[16]{0:T(128)S(1)} %multiply_power_fusion, f32[1024]{0:T(1024)S(1)} %iota_convert_fusion), kind=kLoop, calls=%fused_computation | loop fusion | flops 16384 | bytes 135232 | tf_op jit(solution)/shard_map/sin | solution.py:597
  1.0 89.4 %shard_map.172 = bf16[128,2048]{1,0:T(8,128)(2,1)} custom-call(bf16[128,2048]{1,0:T(8,128)(2,1)} %bitcast.25, bf16[128,1536]{1,0:T(8,128)(2,1)} %bitcast.26, bf16[128,256]{1,0:T(8,128)(2,1)} %bitcast.27, bf16[32,128]{1,0:T(8,128)(2,1)} %bitcast.28, f32[1,256]{1,0:T(1,128)} %bitcast.31, f32[1,96]{1,0:T(1,128)} %bitcast.34, f32[1,96]{1,0:T(1,128)} %bitcast.35, ...), custom_call_target="tpu_custom_call" | custom-call | tf_op jit(solution)/shard_map/pallas_call | solution.py:613
  90.4 1.9 %copy.20 = bf16[1,128,2048]{2,1,0:T(8,128)(2,1)} copy(bf16[1,128,2048]{2,1,0:T(8,128)(2,1)} %bitcast.21) | data formatting | bytes 1048576
  (2 shorter events, 0.0 us)

commit v4 on v3

--- a/solution.py
+++ b/solution.py
@@ -2,6 +2,7 @@
 
 import jax
 import jax.numpy as jnp
+import numpy as np
 from jax import lax
 from jax.experimental import pallas as pl
 from jax.experimental.pallas import tpu as pltpu
@@ -14,10 +15,11 @@
 eps = 1e-06
 
 
-def angles(offset, span_count, rope_width):
-    position = (offset + jnp.arange(span_count, dtype=jnp.int32)).astype(jnp.float32)
-    frequency = 10000.0 ** (-2.0 * jnp.arange(rope_width // 2, dtype=jnp.float32) / rope_width)
-    return position[:, None] * frequency[None, :]
+def turns(length, rope_width):
+    frequency = 10000.0 ** (-2.0 * np.arange(rope_width // 2) / rope_width)
+    position = np.arange(length, dtype=np.float32)
+    phases = (frequency.astype(np.float32)[:, None] * position[None, :]).astype(np.float64)
+    return np.cos(phases).astype(np.float32), np.sin(phases).astype(np.float32)
 
 
 def dot32(a, b):
@@ -209,7 +211,7 @@
     send_first = 1 + (plane + 1) // 2
     send_last = GROUPS - 1 - 2 * (plane // 2)
     send_order = (send_first, 6 - send_first - send_last, send_last)
-    recv_first = 6 - send_first - send_last
+    recv_first = 2 + (1 - plane // 2) * (1 - 2 * (plane % 2))
     recv_last = 1 + 2 * (plane % 2)
     recv_order = (recv_first, 6 - recv_first - recv_last, recv_last)
 
@@ -436,14 +438,17 @@
     stream_ref[...] = stream
     scale = lax.rsqrt(jnp.mean(stream * stream, axis=-1, keepdims=True) + eps)
     normed_ref[...] = (stream * scale * ffn_gain_ref[...]).astype(bf)
+    everyone = jnp.concatenate(
+        [picks[plane]] + [picks[(plane + k) % GROUPS] for k in send_order], axis=0
+    )
+    for c in range(chunks):
+        packed_rows = dot32(everyone, normed_ref[:, span(c)]).astype(bf)
+        in1[0, c] = packed_rows[:rows]
+        for i, k in enumerate(send_order):
+            out1[k, c] = packed_rows[(i + 1) * rows : (i + 2) * rows]
     for k in send_order:
-        chosen = picks[(plane + k) % GROUPS]
         for c in range(chunks):
-            out1[k, c] = dot32(chosen, normed_ref[:, span(c)]).astype(bf)
             first(k, c).start()
-    own = picks[plane]
-    for c in range(chunks):
-        in1[0, c] = dot32(own, normed_ref[:, span(c)]).astype(bf)
 
     def slots(k):
         info = notes[k].astype(jnp.float32)
@@ -490,13 +495,13 @@
         at0, at1, info = slots(k)
         high = jnp.where(at0, info[:, 2:3], 0.0) + jnp.where(at1, info[:, 4:5], 0.0)
         low = jnp.where(at0, info[:, 3:4], 0.0) + jnp.where(at1, info[:, 5:6], 0.0)
-        high = high.astype(bf)
-        low = low.astype(bf)
+        shares = jnp.concatenate([high, low], axis=0).astype(bf)
         for c in range(chunks):
             for j in range(1, peers):
                 third(k, c, j).wait_recv()
             got = back2[k, c].reshape(peers * cap, part)
-            total = (dot32(high, got) + dot32(low, got)).astype(bf)
+            total = dot32(shares, got)
+            total = (total[:rows] + total[rows:]).astype(bf)
             if local:
                 home[0, c] = total
             else:
@@ -505,21 +510,21 @@
 
     scatter(0, True)
     scatter(recv_order[0], False)
+    serve(0, True)
     scatter(recv_order[1], False)
-    serve(recv_order[0], True)
+    serve(recv_order[0], False)
+    scatter(recv_order[2], False)
+    merge(0, True)
     serve(recv_order[1], False)
     merge(recv_order[0], False)
-    scatter(recv_order[2], False)
+    serve(recv_order[2], False)
     merge(recv_order[1], False)
-    serve(recv_order[2], False)
-    serve(0, False)
     merge(recv_order[2], False)
-    merge(0, True)
     for c in range(chunks):
-        total = stream_ref[:, span(c)] + dot_t(own, home[0, c])
         for k in send_order:
             fourth(k, c).wait_recv()
-            total = total + dot_t(picks[(plane + k) % GROUPS], home[k, c])
+        returned = jnp.concatenate([home[0, c]] + [home[k, c] for k in send_order], axis=0)
+        total = stream_ref[:, span(c)] + dot_t(everyone, returned)
         out_ref[:, span(c)] = total.astype(bf)
     for k in range(GROUPS):
         if k:
@@ -580,11 +585,11 @@
     peers = experts // GROUPS
     cap = tok * GROUPS // experts
     rows = peers * cap // expert_choice.shape[2]
-    chunks = 4
+    chunks = 2
     part = width // chunks
     bf = jnp.bfloat16
     f32 = jnp.float32
-    phases = angles(0, n_sp * tok, rope).T
+    cos, sin = turns(n_sp * tok, rope)
     operands = (
         residual[0],
         query[0],
@@ -593,8 +598,8 @@
         latent_gain[None],
         query_gain[None],
         key_gain[None],
-        jnp.cos(phases),
-        jnp.sin(phases),
+        jnp.asarray(cos),
+        jnp.asarray(sin),
         mix_gain[None],
         ffn_gain[None],
         expert_choice[0].T,

time: 92.4 us -> 86.5 us (0.936)
  Pallas kernels: 89.4 us -> 84.4 us
  other arithmetic: 0.99 us -> 0 us
    pallas_call x1, Pallas kernels: 89.4 us -> 84.4 us  [per_device(): pl.pallas_call(functools.partial(layer_kernel, n_sp, n_y, n_dp, heads, no...]
    sin x1 -> x0, other arithmetic: 0.98 us -> none  [per_device(): jnp.sin(phases)]
where the time goes in v4:
time: 86.5 us; the launch traced here: 86.3 us
  Pallas kernels  84.4 us (98%)
  local copies, waits for them, and re-layouts  1.88 us (2%)
    pallas_call x1, Pallas kernels, per_device(): pl.pallas_call(functools.partial(layer_kernel, n_sp, n_y, n_dp, heads, no...  84.4 us
    unnamed x1, local copies, waits for them, and re-layouts  1.88 us

profile of v4, /device:TPU:0, one launch (start us, length us, event | category | flops | bytes accessed | tf_op | source)
XLA Modules:
  0.0 86.3 jit_solution(8140156575300709123)
XLA Ops:
  0.0 84.4 %shard_map.190 = bf16[128,2048]{1,0:T(8,128)(2,1)} custom-call(bf16[128,2048]{1,0:T(8,128)(2,1)} %bitcast.25, bf16[128,1536]{1,0:T(8,128)(2,1)} %bitcast.26, bf16[128,256]{1,0:T(8,128)(2,1)} %bitcast.27, bf16[32,128]{1,0:T(8,128)(2,1)} %bitcast.28, f32[1,256]{1,0:T(1,128)} %bitcast.31, f32[1,96]{1,0:T(1,128)} %bitcast.34, f32[1,96]{1,0:T(1,128)} %bitcast.35, ...), custom_call_target="tpu_custom_call" | custom-call | tf_op jit(solution)/shard_map/pallas_call | solution.py:618
  84.4 1.9 %copy.22 = bf16[1,128,2048]{2,1,0:T(8,128)(2,1)} copy(bf16[1,128,2048]{2,1,0:T(8,128)(2,1)} %bitcast.21) | data formatting | bytes 1048576

commit v5 on v4

--- a/solution.py
+++ b/solution.py
@@ -251,6 +251,43 @@
     packed[me, :tok] = (raw * scale * latent_gain_ref[...]).astype(bf)
     packed[me, tok:, :tok] = rope_ref[:half]
     packed[me, tok:, tok : 2 * tok] = rope_ref[half:]
+    ready(choice_hbm, group_prob_hbm, share_hbm)
+    per_group = peers
+    group = choice_ref[0:1] // per_group
+    order = lax.broadcasted_iota(jnp.int32, (tok, tok), 0)
+    sooner = order < lax.broadcasted_iota(jnp.int32, (tok, tok), 1)
+
+    def tall(line):
+        return jnp.broadcast_to(line.astype(f32), (tok, tok)).T
+
+    def count(flags):
+        return jnp.sum(jnp.where(sooner & flags, 1.0, 0.0), axis=0, keepdims=True)
+
+    rank = count(tall(group) == group.astype(f32))
+    line = group.astype(f32) * rows + rank
+    for g in range(GROUPS):
+        slot = g * rows + lax.broadcasted_iota(jnp.int32, (rows, tok), 0)
+        picks[g] = jnp.where(slot.astype(f32) == line, 1.0, 0.0).astype(bf)
+    talls = (tall(choice_ref[0:1]), tall(choice_ref[1:2]))
+    facts = []
+    for s in range(2):
+        named = choice_ref[s : s + 1].astype(f32)
+        earlier = count(talls[0] == named) + count(talls[1] == named)
+        facts.append((named - group.astype(f32) * per_group) * cap + earlier)
+    total = share_ref[0:1] + share_ref[1:2]
+    for s in range(2):
+        route = group_prob_ref[...] * share_ref[s : s + 1] / total
+        high = route.astype(bf).astype(f32)
+        facts.append(high)
+        facts.append(route - high)
+    facts.append(jnp.zeros((128 - len(facts), tok), f32))
+    facts = jnp.concatenate(facts, axis=0).astype(bf)
+
+    def describe(g):
+        return lax.dot_general(
+            picks[g], facts, (((1,), (1,)), ((), ())), preferred_element_type=f32
+        ).astype(bf)
+
     pl.semaphore_wait(barrier, GROUPS - 1 + peers - 1)
     for k in send_order:
 
@@ -308,43 +345,6 @@
         queries[h] = (y * scale)[:, :qk].astype(bf)
 
 
-    ready(choice_hbm, group_prob_hbm, share_hbm)
-    per_group = peers
-    group = choice_ref[0:1] // per_group
-    order = lax.broadcasted_iota(jnp.int32, (tok, tok), 0)
-    sooner = order < lax.broadcasted_iota(jnp.int32, (tok, tok), 1)
-
-    def tall(line):
-        return jnp.broadcast_to(line.astype(f32), (tok, tok)).T
-
-    def count(flags):
-        return jnp.sum(jnp.where(sooner & flags, 1.0, 0.0), axis=0, keepdims=True)
-
-    rank = count(tall(group) == group.astype(f32))
-    line = group.astype(f32) * rows + rank
-    for g in range(GROUPS):
-        slot = g * rows + lax.broadcasted_iota(jnp.int32, (rows, tok), 0)
-        picks[g] = jnp.where(slot.astype(f32) == line, 1.0, 0.0).astype(bf)
-    talls = (tall(choice_ref[0:1]), tall(choice_ref[1:2]))
-    facts = []
-    for s in range(2):
-        named = choice_ref[s : s + 1].astype(f32)
-        earlier = count(talls[0] == named) + count(talls[1] == named)
-        facts.append((named - group.astype(f32) * per_group) * cap + earlier)
-    total = share_ref[0:1] + share_ref[1:2]
-    for s in range(2):
-        route = group_prob_ref[...] * share_ref[s : s + 1] / total
-        high = route.astype(bf).astype(f32)
-        facts.append(high)
-        facts.append(route - high)
-    facts.append(jnp.zeros((128 - len(facts), tok), f32))
-    facts = jnp.concatenate(facts, axis=0).astype(bf)
-
-    def describe(g):
-        return lax.dot_general(
-            picks[g], facts, (((1,), (1,)), ((), ())), preferred_element_type=f32
-        ).astype(bf)
-
     notes[0] = describe(plane)
     for k in send_order:
         notes_out[k] = describe((plane + k) % GROUPS)
@@ -514,9 +514,9 @@
     scatter(recv_order[1], False)
     serve(recv_order[0], False)
     scatter(recv_order[2], False)
-    merge(0, True)
     serve(recv_order[1], False)
     merge(recv_order[0], False)
+    merge(0, True)
     serve(recv_order[2], False)
     merge(recv_order[1], False)
     merge(recv_order[2], False)

time: 86.5 us -> 86.4 us (level)
  no operation moved by 1% of the time
where the time goes in v5:
time: 86.4 us; the launch traced here: 86.3 us
  Pallas kernels  84.4 us (98%)
  local copies, waits for them, and re-layouts  1.88 us (2%)
    pallas_call x1, Pallas kernels, per_device(): pl.pallas_call(functools.partial(layer_kernel, n_sp, n_y, n_dp, heads, no...  84.4 us
    unnamed x1, local copies, waits for them, and re-layouts  1.88 us

profile of v5, /device:TPU:0, one launch (start us, length us, event | category | flops | bytes accessed | tf_op | source)
XLA Modules:
  0.0 86.3 jit_solution(12845705512010197527)
XLA Ops:
  0.0 84.4 %shard_map.190 = bf16[128,2048]{1,0:T(8,128)(2,1)} custom-call(bf16[128,2048]{1,0:T(8,128)(2,1)} %bitcast.25, bf16[128,1536]{1,0:T(8,128)(2,1)} %bitcast.26, bf16[128,256]{1,0:T(8,128)(2,1)} %bitcast.27, bf16[32,128]{1,0:T(8,128)(2,1)} %bitcast.28, f32[1,256]{1,0:T(1,128)} %bitcast.31, f32[1,96]{1,0:T(1,128)} %bitcast.34, f32[1,96]{1,0:T(1,128)} %bitcast.35, ...), custom_call_target="tpu_custom_call" | custom-call | tf_op jit(solution)/shard_map/pallas_call | solution.py:618
  84.4 1.9 %copy.22 = bf16[1,128,2048]{2,1,0:T(8,128)(2,1)} copy(bf16[1,128,2048]{2,1,0:T(8,128)(2,1)} %bitcast.21) | data formatting | bytes 1048576
